TPU v7x, 32 devices: a whole 2x2x4 slice. The times are simulated.
32 devices in a mesh: ep: 8 (over z, x), tp: 4 (over y, core).
Axes of the slice: x: 2, y: 2, z: 4, core: 2. Of those that a mesh axis runs over, the one named last changes fastest.
Arguments:
- mix_in: bfloat16 [1024, 2048], P('ep'), may hold values from -6 to 6
- mix_gain: float32 [2048], replicated, may hold values from 0.1 to 1.9
- query_weight: bfloat16 [2048, 3072], P(None, 'tp'), may hold values from -0.125 to 0.125
- latent_weight: bfloat16 [2048, 512], replicated, may hold values from -0.125 to 0.125
- rotary_weight: bfloat16 [2048, 64], replicated, may hold values from -0.125 to 0.125
- latent_gain: float32 [512], replicated, may hold values from 0.1 to 1.9
- key_weight: bfloat16 [512, 2048], P(None, 'tp'), may hold values from -0.25 to 0.25
- value_weight: bfloat16 [512, 2048], P(None, 'tp'), may hold values from -0.25 to 0.25
- output_weight: bfloat16 [2048, 2048], P('tp'), may hold values from -0.125 to 0.125
- out_gain: float32 [2048], replicated, may hold values from 0.1 to 1.9
- ffn_in: bfloat16 [1024, 2048], P('ep'), may hold values from -6 to 6
- ffn_gain: float32 [2048], replicated, may hold values from 0.1 to 1.9
- gate_weight: bfloat16 [8, 2048, 1024], P('ep', None, 'tp'), may hold values from -0.375 to 0.375
- up_weight: bfloat16 [8, 2048, 1024], P('ep', None, 'tp'), may hold values from -0.375 to 0.375
- down_weight: bfloat16 [8, 1024, 2048], P('ep', 'tp'), may hold values from -0.046875 to 0.046875
- routes: int32 [1024, 4], P('ep'), may hold values from 0 to 7, all different within a row; in each aligned block of 32 rows (0 to 31, 32 to 63, ...) at most 32 rows name the same one
- route_scores: float32 [1024, 4], P('ep'), may hold values from -6 to 6
Outputs:
- mixed: bfloat16 [1024, 2048], P(('ep', 'tp'))
- moe_out: bfloat16 [1024, 2048], P(('ep', 'tp'))
Inputs may be any that keep to these rules, and one draw needn't show every extreme that they name: `routes`: each row names 4 different experts; in each aligned block of 32 rows no expert is named by more than 32 rows, a bound that some blocks reach.
All inputs are finite; a program needn't handle non-finite values.
Results may differ from a plain program's by a relative error of at most 0.014.
Values may be sent and summed in bfloat16 or wider, within the bound.
A program may use at most 192 MiB of HBM per device.

v0:
```python
import jax
import jax.numpy as jnp
import functools
from jax import lax
from jax.experimental import pallas as pl
from jax.experimental.pallas import tpu as pltpu
from jax.sharding import PartitionSpec as P

NOPE = 128
ROPE = 64
VD = 128


norm_eps = 1e-06
clamp_limit = 7.0
gate_slope = 1.702
rope_base = 10000.0


def rms_rows(rows_in, scales):
    mean_square = jnp.mean(rows_in * rows_in, axis=-1, keepdims=True)
    return rows_in * lax.rsqrt(mean_square + norm_eps) * scales


def rms_columns(columns, scales):
    mean_square = jnp.mean(columns * columns, axis=0, keepdims=True)
    return columns * lax.rsqrt(mean_square + norm_eps) * scales[:, None]


def turn_table(positions):
    inverse = rope_base ** (-jnp.arange(0, ROPE, 2).astype(jnp.float32) / ROPE)
    angle_rows = inverse[:, None] * positions.astype(jnp.float32)[None, :]
    return (jnp.cos(angle_rows), jnp.sin(angle_rows))


def clamped_unit(gate_part, linear):
    gate_part = jnp.minimum(gate_part, clamp_limit)
    linear = jnp.clip(linear, -clamp_limit, clamp_limit)
    return gate_part * jax.nn.sigmoid(gate_slope * gate_part) * (linear + 1.0)


def keep_state(running):
    return running


def local(
    mix_in,
    mix_gain,
    query_weight,
    latent_weight,
    rotary_weight,
    latent_gain,
    key_weight,
    value_weight,
    output_weight,
    out_gain,
    ffn_in,
    ffn_gain,
    gate_weight,
    up_weight,
    down_weight,
    routes,
    route_scores,
):
    row_count = mix_in.shape[0]
    first_row = lax.axis_index("ep") * row_count
    last_row = first_row + row_count - 1
    positions = first_row + jnp.arange(row_count, dtype=jnp.int32)
    normed = rms_rows(mix_in.astype(jnp.float32), mix_gain).astype(jnp.bfloat16)
    head_count = query_weight.shape[1] // (NOPE + ROPE)
    half_rope = ROPE // 2
    cosine, sine_rows = turn_table(positions)
    queries = jnp.dot(normed, query_weight, preferred_element_type=jnp.float32).reshape(
        row_count, head_count, NOPE + ROPE
    )
    query_plain = queries[..., :NOPE].astype(jnp.bfloat16)
    query_cos = cosine.T[:, None, :]
    query_sin = sine_rows.T[:, None, :]
    query_upper = queries[..., NOPE : NOPE + half_rope]
    query_lower = queries[..., NOPE + half_rope :]
    query_turn = jnp.concatenate(
        [
            query_upper * query_cos - query_lower * query_sin,
            query_lower * query_cos + query_upper * query_sin,
        ],
        axis=-1,
    ).astype(jnp.bfloat16)
    across = (((0,), (1,)), ((), ()))
    latent = rms_columns(
        lax.dot_general(latent_weight, normed, across, preferred_element_type=jnp.float32),
        latent_gain,
    ).astype(jnp.bfloat16)
    rot_raw = lax.dot_general(rotary_weight, normed, across, preferred_element_type=jnp.float32)
    rotary_key = jnp.concatenate(
        [
            rot_raw[:half_rope] * cosine - rot_raw[half_rope:] * sine_rows,
            rot_raw[half_rope:] * cosine + rot_raw[:half_rope] * sine_rows,
        ],
        axis=0,
    ).astype(jnp.bfloat16)
    score_scale = (NOPE + ROPE) ** (-0.5)
    contract_first = (((0,), (0,)), ((), ()))

    def expand(latent_block):
        key_block = lax.dot_general(
            key_weight, latent_block, contract_first, preferred_element_type=jnp.float32
        ).astype(jnp.bfloat16)
        value_block = lax.dot_general(
            value_weight, latent_block, contract_first, preferred_element_type=jnp.float32
        ).astype(jnp.bfloat16)
        return (key_block, value_block)

    def attend(key_block, value_block, turn_block):
        key_count = key_block.shape[1]
        key_block = key_block.reshape(head_count, NOPE, key_count)
        value_block = value_block.reshape(head_count, VD, key_count)
        scores = jnp.einsum(
            "ihd,hdj->hij", query_plain, key_block, preferred_element_type=jnp.float32
        )
        scores = scores + jnp.einsum(
            "ihd,dj->hij", query_turn, turn_block, preferred_element_type=jnp.float32
        )
        key_places = jnp.arange(key_count, dtype=jnp.int32)
        allowed = key_places[None, :] <= positions[:, None]
        weights = jnp.where(allowed[None], jnp.exp(scores * score_scale), 0.0)
        weighted = jnp.einsum(
            "hij,hdj->hid",
            weights.astype(jnp.bfloat16),
            value_block,
            preferred_element_type=jnp.float32,
        )
        return (jnp.sum(weights, axis=-1), weighted)

    initial = (
        jnp.zeros((head_count, row_count), jnp.float32),
        jnp.zeros((head_count, row_count, VD), jnp.float32),
    )
    shard_piece = (
        lax.all_gather(latent, "ep", axis=1, tiled=True),
        lax.all_gather(rotary_key, "ep", axis=1, tiled=True),
    )

    def compute_piece(running):
        key_block, value_block = expand(shard_piece[0])
        return attend(key_block, value_block, shard_piece[1])

    totals, weighted = lax.cond(jnp.int32(0) > last_row, keep_state, compute_piece, initial)
    attended = (weighted / totals[..., None]).astype(jnp.bfloat16)
    mixing = output_weight.reshape(head_count, VD, output_weight.shape[1])
    partial_value = jnp.einsum("hid,hde->ie", attended, mixing, preferred_element_type=jnp.float32)
    projected = lax.psum_scatter(
        lax.optimization_barrier(partial_value.astype(jnp.bfloat16))
        .astype(jnp.float32)
        .astype(jnp.bfloat16),
        "tp",
        scatter_dimension=0,
        tiled=True,
    ).astype(jnp.float32)
    mixed = rms_rows(projected, out_gain).astype(jnp.bfloat16)
    tokens = ffn_in.shape[0]
    part_count = lax.axis_size("tp")
    quarter_rows = tokens // part_count
    experts = lax.axis_size("ep")
    choose = routes.shape[1]
    capacity = max(2, 2 * quarter_rows * choose // experts)
    slot_count = capacity * part_count
    tp_index = lax.axis_index("tp")
    normed_b = rms_rows(ffn_in.astype(jnp.float32), ffn_gain).astype(jnp.bfloat16)
    padded = jnp.concatenate([normed_b, jnp.zeros((1, normed_b.shape[1]), jnp.bfloat16)], axis=0)
    gate_share = jax.nn.softmax(route_scores, axis=-1)
    grouped = routes.reshape(part_count, quarter_rows * choose)
    onehot = (grouped[:, :, None] == jnp.arange(experts, dtype=jnp.int32)[None, None, :]).astype(
        jnp.int32
    )
    slot_rank = jnp.sum((jnp.cumsum(onehot, axis=1) - 1) * onehot, axis=2)
    slot_index = jnp.arange(part_count, dtype=jnp.int32)[:, None] * capacity + slot_rank
    place_index = (slot_index * experts + grouped).reshape(-1)
    owners = jnp.arange(tokens * choose, dtype=jnp.int32) // choose
    slot_token = jnp.full((slot_count * experts,), tokens, jnp.int32).at[place_index].set(owners)
    unit_count = gate_weight.shape[2]
    chosen = lax.dynamic_slice_in_dim(
        slot_token, tp_index * capacity * experts, capacity * experts, 0
    )
    outgoing = padded[chosen].reshape(capacity, experts, -1)
    arrived = lax.all_to_all(outgoing, "ep", split_axis=1, concat_axis=1, tiled=True)
    row_block = lax.all_gather(arrived, "tp", axis=0, tiled=True)
    block_slots = row_block.shape[0]
    flat_rows = row_block.reshape(-1, row_block.shape[2])
    gate_part = jnp.dot(flat_rows, gate_weight[0], preferred_element_type=jnp.float32)
    up_part = jnp.dot(flat_rows, up_weight[0], preferred_element_type=jnp.float32)
    hidden = (
        clamped_unit(gate_part, up_part).astype(jnp.bfloat16).reshape(block_slots, -1, unit_count)
    )
    sources = hidden.shape[1]
    hidden_flat = hidden.reshape(slot_count * sources, unit_count)
    partial_value = jnp.dot(hidden_flat, down_weight[0], preferred_element_type=jnp.float32)
    result = lax.psum_scatter(
        lax.optimization_barrier(partial_value.astype(jnp.bfloat16))
        .astype(jnp.float32)
        .astype(jnp.bfloat16),
        "tp",
        scatter_dimension=0,
        tiled=True,
    )
    result = result.reshape(capacity, sources, -1)
    returned = lax.all_to_all(result, "ep", split_axis=1, concat_axis=1, tiled=True)
    back_rows = returned.reshape(capacity * experts, -1)
    own_rank = lax.dynamic_index_in_dim(slot_rank, tp_index, 0, keepdims=False)
    own_expert = lax.dynamic_index_in_dim(grouped, tp_index, 0, keepdims=False)
    picked = (
        back_rows[own_rank * experts + own_expert]
        .astype(jnp.float32)
        .reshape(quarter_rows, choose, -1)
    )
    own_gates = lax.dynamic_slice_in_dim(gate_share, tp_index * quarter_rows, quarter_rows, 0)
    moe_out = jnp.sum(picked * own_gates[:, :, None], axis=1).astype(jnp.bfloat16)
    return (mixed, moe_out)


MESH = pl.DeviceIdType.MESH


def flip(value, bits):
    bit = 1
    while bit <= bits:
        if bits & bit:
            value = value + bit - 2 * bit * ((value // bit) % 2)
        bit *= 2
    return value


def here():
    ep, tp = lax.axis_index("ep"), lax.axis_index("tp")
    return ep // 2, ep % 2, tp // 2, tp % 2


def place(z, x, y, core):
    return {"ep": z * 2 + x, "tp": y * 2 + core}


def greet(partners):
    barrier = pltpu.get_barrier_semaphore()
    for partner in partners:
        pl.semaphore_signal(barrier, inc=1, device_id=partner, device_id_type=MESH)
    pl.semaphore_wait(barrier, len(partners))


def layer_kernel(
    depth, heads, row_ref, side_ref, query_ref, gain_ref, gate_hbm, up_hbm, down_hbm, key_hbm,
    value_hbm, output_hbm, mixed_ref, moe_ref,
    rows_all, side_all, part_ref, work, twin_in, hop_in, direct_in, relay_in, column_in,
    heads_ref, heads_work, heads_twin, heads_in, keys, values, attended, own_total,
    gate_ref, up_ref, down_ref, key_ref, value_ref, output_ref,
    spread_sem, recv_sem, send_sem, twin_sem, square_sem, column_sem, heads_sem, load_sem,
):
    f32, bf16 = jnp.float32, jnp.bfloat16
    ep = lax.axis_index("ep")
    z, x, y, core = here()
    x_next, y_next, twin = place(z, 1 - x, y, core), place(z, x, 1 - y, core), place(z, x, y, 1 - core)
    columns = [place(flip(z, d), x, y, core) for d in range(1, depth)]
    parts, quarter, width = part_ref.shape[1:]
    row_count = parts * quarter
    side_width = side_ref.shape[1]
    latent_width = key_ref.shape[0]
    experts = 2 * depth
    loads = [
        pltpu.make_async_copy(src, dst, load_sem.at[n])
        for n, (src, dst) in enumerate(
            (
                (gate_hbm, gate_ref), (up_hbm, up_ref), (down_hbm, down_ref),
                (key_hbm, key_ref), (value_hbm, value_ref), (output_hbm, output_ref),
            )
        )
    ]
    for load in loads:
        load.start()
    greet(columns + [x_next, y_next, twin])
    spread, started = [], []

    def copies(origin, target, own):
        e, t = origin["ep"], origin["tp"]
        number = len(spread)
        return [
            pltpu.make_async_remote_copy(
                src_ref=held if own else out.at[e, t],
                dst_ref=out.at[e, t],
                send_sem=spread_sem.at[a, number],
                recv_sem=recv_sem.at[a, e, t],
                device_id=target,
                device_id_type=MESH,
            )
            for a, (held, out) in enumerate(((side_ref, side_all), (row_ref, rows_all)))
        ]

    def give(origin, target, own=False):
        pair = copies(origin, target, own)
        for copy in pair:
            copy.start()
        spread.append(pair)

    def take(origin):
        for copy in copies(origin, twin, False):
            copy.wait_recv()

    def make(src, dst, sem, target):
        return pltpu.make_async_remote_copy(
            src_ref=src, dst_ref=dst, send_sem=send_sem.at[len(started)], recv_sem=sem,
            device_id=target, device_id_type=MESH,
        )

    def send(src, dst, sem, target):
        copy = make(src, dst, sem, target)
        copy.start()
        started.append(copy)

    def arrive(dst, sem):
        make(dst, dst, sem, twin).wait_recv()

    def forward_column(d):
        origin = place(flip(z, d), x, y, core)
        take(origin)
        for target in (x_next, y_next, twin):
            give(origin, target)

    def forward_square(d):
        at = flip(z, d)
        from_x, from_y = place(at, 1 - x, y, core), place(at, x, 1 - y, core)
        take(from_x)
        if d % 2 == 0:
            give(from_x, y_next)
        give(from_x, twin)
        take(from_y)
        if d % 2 == 1:
            give(from_y, x_next)
        give(from_y, twin)

    def forward_corner(d):
        origin = place(flip(z, d), 1 - x, 1 - y, core)
        take(origin)
        give(origin, twin)

    def side_block(e):
        return side_all[e].reshape(row_count, side_width)

    lane = lax.broadcasted_iota(jnp.int32, (row_count, side_width - latent_width), 1)
    is_mine = (lane == ROPE + ep) | (lane == ROPE + experts + ep)

    def expert_plane(d):
        for a in (0, 1):
            for b in (0, 1):
                take(place(flip(z, d), flip(x, a), flip(y, b), 1 - core))

        @pl.loop(0, 2)
        def _(i):
            e = flip(z, d) * 2 + i
            block = rows_all[e].reshape(row_count, width)
            gate_part = jnp.dot(block, gate_ref[...], preferred_element_type=f32)
            up_part = jnp.dot(block, up_ref[...], preferred_element_type=f32)
            hidden = clamped_unit(gate_part, up_part).astype(bf16)
            table = side_block(e)[:, latent_width:].astype(f32)
            share = jnp.sum(jnp.where(is_mine, table, 0.0), axis=1, keepdims=True)
            chunk = 512
            for n in range(0, width, chunk):
                piece = jnp.dot(hidden, down_ref[:, n : n + chunk], preferred_element_type=f32) * share
                part_ref[e, :, :, n : n + chunk] = piece.astype(bf16).reshape(parts, quarter, chunk)

        for a, b in ((1, 1), (1, 0), (0, 1), (0, 0)):
            e, t = flip(z, d) * 2 + flip(x, a), flip(y, b) * 2 + 1 - core
            send(part_ref.at[e, t], twin_in.at[d, a, b], twin_sem.at[d, a, b], twin)

    def paired(d, a, b):
        arrive(twin_in.at[d, a, b], twin_sem.at[d, a, b])
        own = part_ref[flip(z, d) * 2 + flip(x, a), flip(y, b) * 2 + core]
        return own.astype(f32) + twin_in[d, a, b].astype(f32)

    def sum_pairs(d):
        work[d, 1, 1] = paired(d, 1, 1).astype(bf16)
        send(work.at[d, 1, 1], hop_in.at[d], square_sem.at[0, d], y_next if d % 2 else x_next)
        a, b = (0, 1) if d % 2 else (1, 0)
        work[d, a, b] = paired(d, a, b).astype(bf16)
        send(work.at[d, a, b], direct_in.at[d], square_sem.at[1, d], y_next if d % 2 else x_next)

    def sum_relay(d):
        a, b = (1, 0) if d % 2 else (0, 1)
        value = paired(d, a, b)
        arrive(hop_in.at[d], square_sem.at[0, d])
        work[d, a, b] = (value + hop_in[d].astype(f32)).astype(bf16)
        send(work.at[d, a, b], relay_in.at[d], square_sem.at[2, d], x_next if d % 2 else y_next)

    def sum_square(d):
        value = paired(d, 0, 0)
        arrive(direct_in.at[d], square_sem.at[1, d])
        value = value + direct_in[d].astype(f32)
        arrive(relay_in.at[d], square_sem.at[2, d])
        value = value + relay_in[d].astype(f32)
        if d:
            work[d, 0, 0] = value.astype(bf16)
            send(work.at[d, 0, 0], column_in.at[d], column_sem.at[d], columns[d - 1])
        else:
            own_total[...] = value

    across = (((1,), (1,)), ((), ()))
    score_scale = (NOPE + ROPE) ** (-0.5)

    def expand():
        @pl.loop(0, experts)
        def _(e):
            block = side_block(e)
            latent, rest = block[:, :latent_width], block[:, latent_width:]
            at = pl.ds(pl.multiple_of(e * row_count, row_count), row_count)
            key_block = jnp.dot(latent, key_ref[...], preferred_element_type=f32).astype(bf16)
            value_block = jnp.dot(latent, value_ref[...], preferred_element_type=f32).astype(bf16)
            for h in range(heads):
                keys[h, at, :NOPE] = key_block[:, h * NOPE : (h + 1) * NOPE]
                keys[h, at, NOPE:] = rest
                values[h, at, :] = value_block[:, h * VD : (h + 1) * VD]

    def attend(h):
        tokens = experts * row_count
        chunk = 256
        totals = jnp.zeros((row_count, 1), f32)
        weighted = jnp.zeros((row_count, VD), f32)
        places = lax.broadcasted_iota(jnp.int32, (row_count, chunk), 0) + ep * row_count
        for n in range(0, tokens, chunk):
            scores = lax.dot_general(
                query_ref[h], keys[h, n : n + chunk, :], across, preferred_element_type=f32
            )
            allowed = lax.broadcasted_iota(jnp.int32, (row_count, chunk), 1) + n <= places
            weights = jnp.where(allowed, jnp.exp(scores * score_scale), 0.0)
            totals = totals + jnp.sum(weights, axis=1, keepdims=True)
            weighted = weighted + jnp.dot(
                weights.astype(bf16), values[h, n : n + chunk, :], preferred_element_type=f32
            )
        attended[:, h * VD : (h + 1) * VD] = (weighted / totals).astype(bf16)

    def project():
        chunk = 512
        for n in range(0, width, chunk):
            piece = jnp.dot(attended[...], output_ref[:, n : n + chunk], preferred_element_type=f32)
            heads_ref[:, :, n : n + chunk] = piece.astype(bf16).reshape(parts, quarter, chunk)
        for b in (1, 0):
            send(heads_ref.at[flip(y, b) * 2 + 1 - core], heads_twin.at[b], heads_sem.at[b], twin)

    me = place(z, x, y, core)
    for target in columns + [x_next, y_next, twin]:
        give(me, target, True)
    rows_all[me["ep"], me["tp"]] = row_ref[...]
    side_all[me["ep"], me["tp"]] = side_ref[...]
    for load in loads:
        load.wait()

    def reduce_after(last):
        for step, back in ((sum_pairs, 0), (sum_relay, 1), (sum_square, 2)):
            if 0 <= last - back < depth:
                step(last - back)

    for d in range(1, depth + 3):
        if d < depth:
            forward_column(d)
        if d - 1 < depth:
            forward_square(d - 1)
        if 0 <= d - 2 < depth:
            forward_corner(d - 2)
        if 0 <= d - 3 < depth:
            expert_plane(d - 3)
        if 0 <= d - 4:
            reduce_after(d - 4)
    expand()
    reduce_after(depth - 1)
    for h in range(heads):
        attend(h)
        if h % 2 == 0 and h < 4:
            reduce_after(depth + h // 2)
    for h in range((heads + 1) // 2, 2):
        reduce_after(depth + h)
    project()
    arrive(heads_twin.at[1], heads_sem.at[1])
    heads_work[...] = (
        heads_ref[(1 - y) * 2 + core].astype(f32) + heads_twin[1].astype(f32)
    ).astype(bf16)
    send(heads_work, heads_in, heads_sem.at[2], y_next)
    total = own_total[...]
    for d in range(1, depth):
        arrive(column_in.at[d], column_sem.at[d])
        total = total + column_in[d].astype(f32)
    moe_ref[...] = total.astype(bf16)
    arrive(heads_twin.at[0], heads_sem.at[0])
    arrive(heads_in, heads_sem.at[2])
    projected = (
        heads_ref[y * 2 + core].astype(f32) + heads_twin[0].astype(f32) + heads_in[...].astype(f32)
    )
    mixed_ref[...] = rms_rows(projected, gain_ref[...]).astype(bf16)
    for copy in started:
        copy.wait_send()
    for pair in spread:
        for copy in pair:
            copy.wait_send()


def layer(rows, side, queries, gain, weights, experts, parts):
    depth, heads = experts // 2, queries.shape[0]
    quarter, width = rows.shape
    row_count = quarter * parts
    tokens = experts * row_count
    vmem, anywhere = pl.BlockSpec(memory_space=pltpu.VMEM), pl.BlockSpec(memory_space=pl.ANY)
    held = lambda *lead: pltpu.VMEM(lead + (quarter, width), jnp.bfloat16)
    scratch = lambda *shape: pltpu.VMEM(shape, jnp.bfloat16)
    sems = lambda *shape: pltpu.SemaphoreType.DMA(shape)
    gives = depth + 2 + 3 * (depth - 1) + 3 * depth + depth
    return pl.pallas_call(
        functools.partial(layer_kernel, depth, heads),
        out_shape=[jax.ShapeDtypeStruct((quarter, width), jnp.bfloat16)] * 2,
        in_specs=[vmem] * 4 + [anywhere] * len(weights),
        out_specs=[vmem] * 2,
        scratch_shapes=[
            held(experts, parts), scratch(experts, parts, quarter, side.shape[1]),
            held(experts, parts), held(depth, 2, 2), held(depth, 2, 2),
            held(depth), held(depth), held(depth), held(depth),
            held(parts), held(), held(2), held(),
            scratch(heads, tokens, queries.shape[2]), scratch(heads, tokens, VD),
            scratch(row_count, heads * VD), pltpu.VMEM((quarter, width), jnp.float32),
        ]
        + [scratch(*w.shape) for w in weights]
        + [
            sems(2, gives + 1), sems(2, experts, parts), sems(3 + 8 * depth), sems(depth, 2, 2),
            sems(3, depth), sems(depth), sems(3), sems(len(weights)),
        ],
        compiler_params=pltpu.CompilerParams(
            collective_id=0, has_side_effects=True, vmem_limit_bytes=56 * 1024 * 1024
        ),
        name="layer",
    )(rows, side, queries, gain.reshape(1, -1), *weights)


def dense_local(
    mix_in, mix_gain, query_weight, latent_weight, rotary_weight, latent_gain, key_weight,
    value_weight, output_weight, out_gain, ffn_in, ffn_gain, gate_weight, up_weight, down_weight,
    routes, route_scores,
):
    f32, bf16 = jnp.float32, jnp.bfloat16
    experts, parts = lax.axis_size("ep"), lax.axis_size("tp")
    ep, tp = lax.axis_index("ep"), lax.axis_index("tp")
    row_count, width = mix_in.shape
    quarter = row_count // parts
    latent_width = latent_weight.shape[1]
    half = ROPE // 2
    first_row = ep * row_count

    def own(array):
        return lax.dynamic_slice_in_dim(array, tp * quarter, quarter, 0)

    rows = rms_rows(own(ffn_in).astype(f32), ffn_gain).astype(bf16)
    own_normed = rms_rows(own(mix_in).astype(f32), mix_gain).astype(bf16)
    latent = rms_rows(jnp.dot(own_normed, latent_weight, preferred_element_type=f32), latent_gain)
    turned = jnp.dot(own_normed, rotary_weight, preferred_element_type=f32)
    positions = first_row + jnp.arange(row_count, dtype=jnp.int32)
    inverse = rope_base ** (-jnp.arange(0, ROPE, 2).astype(f32) / ROPE)
    angles = positions.astype(f32)[:, None] * inverse[None, :]
    cosine, sine = jnp.cos(angles), jnp.sin(angles)

    def rotate(vectors, cosine, sine):
        upper, lower = vectors[..., :half], vectors[..., half:]
        return jnp.concatenate([upper * cosine - lower * sine, lower * cosine + upper * sine], axis=-1)

    rotary_key = rotate(turned, own(cosine), own(sine))
    shares = jax.nn.softmax(own(route_scores), axis=-1)
    named = own(routes)[:, :, None] == jnp.arange(experts, dtype=jnp.int32)[None, None, :]
    table = jnp.sum(jnp.where(named, shares[:, :, None], 0.0), axis=1)
    coarse = lax.reduce_precision(table, 8, 7)
    used = latent_width + ROPE + 2 * experts
    side_width = -(-used // 128) * 128
    side = jnp.concatenate(
        [latent, rotary_key, coarse, table - coarse, jnp.zeros((quarter, side_width - used), f32)],
        axis=1,
    ).astype(bf16)
    normed = rms_rows(mix_in.astype(f32), mix_gain).astype(bf16)
    head_count = query_weight.shape[1] // (NOPE + ROPE)
    queries = jnp.dot(normed, query_weight, preferred_element_type=f32).reshape(
        row_count, head_count, NOPE + ROPE
    )
    query_turn = rotate(queries[..., NOPE:], cosine[:, None, :], sine[:, None, :])
    spare = jnp.zeros((row_count, head_count, side_width - latent_width - ROPE), f32)
    queries = jnp.concatenate([queries[..., :NOPE], query_turn, spare], axis=-1)
    queries = queries.astype(bf16).transpose(1, 0, 2)
    weights = (
        gate_weight[0], up_weight[0], down_weight[0], key_weight, value_weight, output_weight
    )
    mixed, moe_out = layer(rows, side, queries, out_gain, weights, experts, parts)
    return mixed, moe_out


def solution(mesh):
    experts, parts = mesh.shape["ep"], mesh.shape["tp"]

    def body(*args):
        quarter, choose = args[10].shape[0] // parts, args[15].shape[1]
        every_row = 2 * quarter * choose >= quarter * experts
        paired = parts == 4 and experts % 2 == 0 and (experts // 2) & (experts // 2 - 1) == 0
        return (dense_local if every_row and paired else local)(*args)
    placed = (
        P("ep", None),
        P(),
        P(None, "tp"),
        P(),
        P(),
        P(),
        P(None, "tp"),
        P(None, "tp"),
        P("tp", None),
        P(),
        P("ep", None),
        P(),
        P("ep", None, "tp"),
        P("ep", None, "tp"),
        P("ep", "tp", None),
        P("ep", None),
        P("ep", None),
    )
    return jax.shard_map(
        body,
        mesh=mesh,
        in_specs=placed,
        out_specs=(P(("ep", "tp"), None), P(("ep", "tp"), None)),
        check_vma=False,
    )
```

profile of v0, /device:TPU:0, one launch (start us, length us, event | category | flops | bytes accessed | tf_op | source)
XLA Modules:
  0.0 94.4 jit_solution(7755099988289293396)
XLA Ops:
  0.6 0.0 copy-start
  0.6 0.0 copy-start.4
  0.7 0.0 copy-start.5
  0.7 0.9 fusion.21
  1.6 0.8 fusion.18
  2.4 0.0 copy-start.3
  2.4 1.2 %fusion = f32[128]{0:T(128)S(1)} fusion(bf16[128,2048]{1,0:T(8,128)(2,1)} %param.17), kind=kLoop, calls=%fused_computation.2 | loop fusion | flops 786304 | bytes 524800 | tf_op jit(solution)/shard_map/reduce_sum | solution.py:21
  3.7 0.1 pad.3.clone
  3.8 0.8 fusion.17
  4.5 1.1 %fusion.7 = (f32[32]{0:T(128)S(1)}, f32[32]{0:T(128)S(1)}) fusion(bf16[128,2048]{1,0:T(8,128)(2,1)} %param.27, s32[]{:T(128)S(6)} %select_n.5, bf16[128,2048]{1,0:T(8,128)(2,1)} %param.17), kind=kLoop, calls=%fused_computation.12 | loop fusion | flops 393152 | bytes 262404 | tf_op jit(solution)/shard_map/reduce_sum | solution.py:21
  5.7 0.8 constant_dynamic-slice_fusion.1
  6.5 0.1 copy.34
  6.5 0.1 copy.33
  6.6 1.3 %fusion.13 = f32[32,64]{1,0:T(8,128)S(1)} fusion(bf16[2048,64]{0,1:T(8,128)(2,1)} %param.21, f32[2048]{0:T(1024)} %param.18, f32[32]{0:T(128)S(1)} %add_rsqrt_fusion.2, bf16[128,2048]{1,0:T(8,128)(2,1)} %param.17, s32[]{:T(128)S(6)} %select_n.5), kind=kOutput, calls=%fused_computation.26 | convolution fusion | flops 8650752 | bytes 409732 | tf_op jit(solution)/shard_map/dot_general | solution.py:555
  7.9 2.3 %multiply_reduce_fusion = (f32[32]{0:T(128)S(1)}, f32[32,512]{1,0:T(8,128)S(1)}) fusion(bf16[2048,512]{1,0:T(8,128)(2,1)} %param.20, f32[2048]{0:T(1024)} %param.18, f32[32]{0:T(128)S(1)} %add_rsqrt_fusion.2, bf16[128,2048]{1,0:T(8,128)(2,1)} %param.17, s32[]{:T(128)S(6)} %select_n.5), kind=kOutput, calls=%fused_computation.25 | convolution fusion | flops 67403744 | bytes 2302212 | tf_op jit(solution)/shard_map/dot_general | solution.py:554
  10.2 0.0 copy-done.5
  10.3 0.1 multiply_convert_fusion
  10.3 0.3 multiply_cosine_fusion
  10.7 0.0 copy-start.1
  10.7 0.0 copy-start.2
  10.7 0.6 copy-done.1
  11.3 0.1 add_convert_fusion.1
  11.4 0.0 copy-done.2
  11.4 0.7 concatenate.8.side_ref
  12.1 0.0 copy-done.4
  12.1 1.7 %fusion.9.row_ref = bf16[32,2048]{1,0:T(8,128)(2,1)} fusion(f32[2048]{0:T(1024)S(1)} %copy-done.4, f32[32]{0:T(128)S(1)} %add_rsqrt_fusion.3, bf16[128,2048]{1,0:T(8,128)(2,1)} %param.27, s32[]{:T(128)S(6)} %select_n.5), kind=kLoop, calls=%fused_computation.14 | loop fusion | flops 262144 | bytes 270468 | tf_op jit(solution)/shard_map/convert_element_type | solution.py:552
  13.7 0.0 copy-done
  13.7 0.0 copy-done.3
  13.7 2.4 %fusion.3 = f32[128,768]{0,1:T(8,128)S(1)} fusion(bf16[2048,768]{1,0:T(8,128)(2,1)S(1)} %copy-done, bf16[128,2048]{1,0:T(8,128)(2,1)} %param.17, f32[2048]{0:T(1024)S(1)} %copy-done.3, f32[128]{0:T(128)S(1)} %add_rsqrt_fusion), kind=kOutput, calls=%fused_computation.5 | convolution fusion | flops 403701760 | bytes 4071936 | tf_op jit(solution)/shard_map/dot_general | solution.py:578
  16.2 0.6 fusion.22
  16.8 0.1 copy.41
  17.0 1.0 %copy.43 = f32[128,4,32]{2,0,1:T(8,128)S(1)} copy(f32[128,4,32]{0,2,1:T(8,128)} %get-tuple-element.4) | data formatting | bytes 131072
  18.0 1.7 %copy.42 = f32[128,4,32]{2,0,1:T(8,128)} copy(f32[128,4,32]{0,2,1:T(8,128)} %get-tuple-element.5) | data formatting | bytes 131072
  19.6 1.1 %subtract_convert_fusion = (bf16[128,4,32]{2,0,1:T(8,128)(2,1)S(1)}, bf16[128,4,32]{2,0,1:T(8,128)(2,1)S(1)}) fusion(f32[128,4,32]{2,0,1:T(8,128)S(1)} %copy.43, f32[128,4,32]{2,0,1:T(8,128)} %copy.42, f32[128,32]{1,0:T(8,128)} %copy-done.2, f32[128,32]{1,0:T(8,128)} %copy-done.1), kind=kLoop, calls=%fused_computation.21 | loop fusion | flops 131072 | bytes 229376 | tf_op jit(solution)/shard_map/convert.1
  20.7 0.8 maximum_bitcast_fusion.query_ref
  21.5 69.8 %layer.1 = (bf16[32,2048]{1,0:T(8,128)(2,1)}, bf16[32,2048]{1,0:T(8,128)(2,1)}) custom-call(bf16[32,2048]{1,0:T(8,128)(2,1)} %fusion.9.row_ref, bf16[32,640]{1,0:T(8,128)(2,1)} %concatenate.8.side_ref, bf16[4,128,256]{2,1,0:T(8,128)(2,1)} %maximum_bitcast_fusion.query_ref, f32[1,2048]{1,0:T(1,128)} %bitcast.15, bf16[2048,256]{1,0:T(8,128)(2,1)} %bitcast.12, ...), custom_call_target="tpu_custom_call" | custom-call | tf_op jit(solution)/shard_map/layer/pallas_call | solution.py:510
  91.3 1.6 %copy.46 = bf16[32,2048]{1,0:T(8,128)(2,1)} copy(bf16[32,2048]{1,0:T(8,128)(2,1)} %get-tuple-element.18) | data formatting | bytes 262144
  92.8 1.6 %copy.47 = bf16[32,2048]{1,0:T(8,128)(2,1)} copy(bf16[32,2048]{1,0:T(8,128)(2,1)} %get-tuple-element.19) | data formatting | bytes 262144
  (12 shorter events, 0.1 us)
Async XLA Ops:
  0.6 13.1 %copy-start = (bf16[2048,768]{1,0:T(8,128)(2,1)S(1)}, bf16[2048,768]{1,0:T(8,128)(2,1)}, u32[]{:S(2)}) copy-start(bf16[2048,768]{1,0:T(8,128)(2,1)} %param.19) | copy-start | bytes 9437188
  0.6 11.4 %copy-start.4 = (f32[2048]{0:T(1024)S(1)}, f32[2048]{0:T(1024)}, u32[]{:S(2)}) copy-start(f32[2048]{0:T(1024)} %param.28) | copy-start | bytes 24580
  0.7 9.6 %copy-start.5 = (f32[512]{0:T(512)S(1)}, f32[512]{0:T(512)}, u32[]{:S(2)}) copy-start(f32[512]{0:T(512)} %param.22) | copy-start | bytes 6148
  2.4 11.3 %copy-start.3 = (f32[2048]{0:T(1024)S(1)}, f32[2048]{0:T(1024)}, u32[]{:S(2)}) copy-start(f32[2048]{0:T(1024)} %param.18) | copy-start | bytes 24580
  10.7 0.6 copy-start.1
  10.7 0.7 copy-start.2
where the time goes:
time: 94.9 us; the launch traced here: 94.4 us
  Pallas kernels  69.8 us (74%)
  local copies, waits for them, and re-layouts  8.91 us (9%)
  other arithmetic  8.91 us (9%)
  matrix products  6.03 us (6%)
    pallas_call x1, Pallas kernels, layer(): pl.pallas_call(functools.partial(layer_kernel, depth, heads), out_shape=[...  69.8 us
    unnamed x17, local copies, waits for them, and re-layouts  6.54 us
    dot_general x1, matrix products, dense_local(): jnp.dot(normed, query_weight, preferred_element_type=f32)  2.41 us
    reduce_sum x2, other arithmetic, rms_rows(): mean_square = jnp.mean(rows_in * rows_in, axis=-1, keepdims=True)  2.38 us
    dot_general x1, matrix products, dense_local(): jnp.dot(own_normed, latent_weight, preferred_element_type=f32)  2.32 us

commit v1 on v0

--- a/solution.py
+++ b/solution.py
@@ -1,6 +1,7 @@
 import jax
 import jax.numpy as jnp
 import functools
+import numpy as np
 from jax import lax
 from jax.experimental import pallas as pl
 from jax.experimental.pallas import tpu as pltpu
@@ -246,34 +247,46 @@
 
 
 def layer_kernel(
-    depth, heads, row_ref, side_ref, query_ref, gain_ref, gate_hbm, up_hbm, down_hbm, key_hbm,
+    depth, heads, side_width,
+    ffn_hbm, mix_hbm, ffn_gain_hbm, mix_gain_hbm, latent_gain_hbm, out_gain_hbm, routes_hbm, scores_hbm,
+    base_hbm, step_hbm, latent_hbm, rotary_hbm, query_hbm, gate_hbm, up_hbm, down_hbm, key_hbm,
     value_hbm, output_hbm, mixed_ref, moe_ref,
+    row_ref, side_ref, query_ref,
     rows_all, side_all, part_ref, work, twin_in, hop_in, direct_in, relay_in, column_in,
-    heads_ref, heads_work, heads_twin, heads_in, keys, values, attended, own_total,
-    gate_ref, up_ref, down_ref, key_ref, value_ref, output_ref,
+    heads_ref, heads_work, heads_twin, heads_in, keys, values, attended, own_total, table_ref, turn_ref,
+    ffn_ref, mix_ref, ffn_gain, mix_gain, latent_gain, gain_ref, routes_ref, scores_ref,
+    base_ref, step_ref, latent_ref, rotary_ref, query_w, gate_ref, up_ref, down_ref, key_ref, value_ref, output_ref,
     spread_sem, recv_sem, send_sem, twin_sem, square_sem, column_sem, heads_sem, load_sem,
 ):
     f32, bf16 = jnp.float32, jnp.bfloat16
-    ep = lax.axis_index("ep")
+    ep, tp = lax.axis_index("ep"), lax.axis_index("tp")
     z, x, y, core = here()
     x_next, y_next, twin = place(z, 1 - x, y, core), place(z, x, 1 - y, core), place(z, x, y, 1 - core)
     columns = [place(flip(z, d), x, y, core) for d in range(1, depth)]
     parts, quarter, width = part_ref.shape[1:]
     row_count = parts * quarter
-    side_width = side_ref.shape[1]
     latent_width = key_ref.shape[0]
     experts = 2 * depth
-    loads = [
-        pltpu.make_async_copy(src, dst, load_sem.at[n])
-        for n, (src, dst) in enumerate(
-            (
-                (gate_hbm, gate_ref), (up_hbm, up_ref), (down_hbm, down_ref),
-                (key_hbm, key_ref), (value_hbm, value_ref), (output_hbm, output_ref),
-            )
-        )
-    ]
+    half = ROPE // 2
+    first_own = pl.multiple_of(tp * quarter, quarter)
+    pairs = (
+        (ffn_hbm.at[pl.ds(first_own, quarter)], ffn_ref), (ffn_gain_hbm, ffn_gain),
+        (mix_hbm, mix_ref), (mix_gain_hbm, mix_gain), (latent_hbm, latent_ref), (rotary_hbm, rotary_ref),
+        (latent_gain_hbm, latent_gain), (base_hbm, base_ref), (step_hbm, step_ref),
+        (routes_hbm, routes_ref), (scores_hbm, scores_ref), (query_hbm, query_w),
+        (gate_hbm, gate_ref), (up_hbm, up_ref), (down_hbm, down_ref),
+        (key_hbm, key_ref), (value_hbm, value_ref), (output_hbm, output_ref), (out_gain_hbm, gain_ref),
+    )
+    loads = [pltpu.make_async_copy(src, dst, load_sem.at[n]) for n, (src, dst) in enumerate(pairs)]
     for load in loads:
         load.start()
+    waited = [0]
+
+    def loaded(count):
+        while waited[0] < count:
+            loads[waited[0]].wait()
+            waited[0] += 1
+
     greet(columns + [x_next, y_next, twin])
     spread, started = [], []
 
@@ -289,11 +302,11 @@
                 device_id=target,
                 device_id_type=MESH,
             )
-            for a, (held, out) in enumerate(((side_ref, side_all), (row_ref, rows_all)))
+            for a, (held, out) in enumerate(((row_ref, rows_all), (side_ref, side_all)))
         ]
 
-    def give(origin, target, own=False):
-        pair = copies(origin, target, own)
+    def give(origin, target):
+        pair = copies(origin, target, False)
         for copy in pair:
             copy.start()
         spread.append(pair)
@@ -342,28 +355,24 @@
     def side_block(e):
         return side_all[e].reshape(row_count, side_width)
 
-    lane = lax.broadcasted_iota(jnp.int32, (row_count, side_width - latent_width), 1)
-    is_mine = (lane == ROPE + ep) | (lane == ROPE + experts + ep)
-
     def expert_plane(d):
         for a in (0, 1):
             for b in (0, 1):
                 take(place(flip(z, d), flip(x, a), flip(y, b), 1 - core))
-
-        @pl.loop(0, 2)
-        def _(i):
-            e = flip(z, d) * 2 + i
-            block = rows_all[e].reshape(row_count, width)
-            gate_part = jnp.dot(block, gate_ref[...], preferred_element_type=f32)
-            up_part = jnp.dot(block, up_ref[...], preferred_element_type=f32)
-            hidden = clamped_unit(gate_part, up_part).astype(bf16)
-            table = side_block(e)[:, latent_width:].astype(f32)
-            share = jnp.sum(jnp.where(is_mine, table, 0.0), axis=1, keepdims=True)
-            chunk = 512
-            for n in range(0, width, chunk):
-                piece = jnp.dot(hidden, down_ref[:, n : n + chunk], preferred_element_type=f32) * share
-                part_ref[e, :, :, n : n + chunk] = piece.astype(bf16).reshape(parts, quarter, chunk)
-
+        first = flip(z, d) * 2
+        pair = pl.ds(first, 2)
+        block = rows_all[pair].reshape(2 * row_count, width)
+        gate_part = jnp.dot(block, gate_ref[...], preferred_element_type=f32)
+        up_part = jnp.dot(block, up_ref[...], preferred_element_type=f32)
+        hidden = clamped_unit(gate_part, up_part).astype(bf16)
+        table = side_all[pair, :, :, latent_width:].reshape(2 * row_count, side_width - latent_width)
+        lane = lax.broadcasted_iota(jnp.int32, table.shape, 1)
+        is_mine = (lane == ROPE + ep) | (lane == ROPE + experts + ep)
+        share = jnp.sum(jnp.where(is_mine, table.astype(f32), 0.0), axis=1, keepdims=True)
+        chunk = 512
+        for n in range(0, width, chunk):
+            piece = jnp.dot(hidden, down_ref[:, n : n + chunk], preferred_element_type=f32) * share
+            part_ref[pair, :, :, n : n + chunk] = piece.astype(bf16).reshape(2, parts, quarter, chunk)
         for a, b in ((1, 1), (1, 0), (0, 1), (0, 0)):
             e, t = flip(z, d) * 2 + flip(x, a), flip(y, b) * 2 + 1 - core
             send(part_ref.at[e, t], twin_in.at[d, a, b], twin_sem.at[d, a, b], twin)
@@ -402,12 +411,78 @@
     across = (((1,), (1,)), ((), ()))
     score_scale = (NOPE + ROPE) ** (-0.5)
 
+    def angles():
+        near, far = base_ref[...], step_ref[pl.ds(ep, 1), :]
+        swapped = pltpu.roll(near, ROPE, 1)
+        lane = lax.broadcasted_iota(jnp.int32, near.shape, 1)
+        cosine, sine = jnp.where(lane < ROPE, near, swapped), jnp.where(lane < ROPE, swapped, near)
+        far_swapped = pltpu.roll(jnp.broadcast_to(far, near.shape), ROPE, 1)
+        far = jnp.broadcast_to(far, near.shape)
+        far_cos, far_sin = jnp.where(lane < ROPE, far, far_swapped), jnp.where(lane < ROPE, far_swapped, far)
+        turn_ref[...] = jnp.where(
+            lane < ROPE, cosine * far_cos - sine * far_sin, sine * far_cos + cosine * far_sin
+        )
+
+    def rotate(vectors, table):
+        lane = lax.broadcasted_iota(jnp.int32, vectors.shape, 1)
+        size = vectors.shape[1]
+        turned = jnp.where(
+            lane < half, -pltpu.roll(vectors, size - half, 1), pltpu.roll(vectors, half, 1)
+        )
+        sine = pltpu.roll(table, size - ROPE, 1)
+        return jnp.where(lane < ROPE, vectors * table + turned * sine, 0.0)
+
+    def prepare_rows():
+        loaded(2)
+        row_ref[...] = rms_rows(ffn_ref[...].astype(f32), ffn_gain[...]).astype(bf16)
+
+    def prepare_side():
+        loaded(11)
+        own = pl.ds(first_own, quarter)
+        normed = rms_rows(mix_ref[own, :].astype(f32), mix_gain[...]).astype(bf16)
+        latent = jnp.dot(normed, latent_ref[...], preferred_element_type=f32)
+        side_ref[:, :latent_width] = rms_rows(latent, latent_gain[...]).astype(bf16)
+        angles()
+        turned = lax.dot_general(normed, rotary_ref[...], across, preferred_element_type=f32)
+        spare = side_width - latent_width - ROPE
+        turned = jnp.concatenate([turned, jnp.zeros((quarter, spare), f32)], axis=1)
+        rotary_key = rotate(turned, turn_ref[own, :])
+        scores = scores_ref[...]
+        shares = jnp.exp(scores - jnp.max(scores, axis=0, keepdims=True))
+        shares = shares / jnp.sum(shares, axis=0, keepdims=True)
+        routes = routes_ref[...]
+        lane = lax.broadcasted_iota(jnp.int32, (side_width - latent_width, row_count), 0)
+        named = jnp.zeros((side_width - latent_width, row_count), f32)
+        for k in range(routes.shape[0]):
+            hit = (lane == routes[k : k + 1] + ROPE) | (lane == routes[k : k + 1] + ROPE + experts)
+            named = named + jnp.where(hit, shares[k : k + 1], 0.0)
+        coarse = named.astype(bf16).astype(f32)
+        table_ref[...] = jnp.where(lane < ROPE + experts, coarse, named - coarse).T
+        side_ref[:, latent_width:] = (rotary_key + table_ref[own, :]).astype(bf16)
+
+    def prepare_queries():
+        loaded(12)
+        normed = rms_rows(mix_ref[...].astype(f32), mix_gain[...]).astype(bf16)
+        plain_and_turn = NOPE + ROPE
+        for h in range(0, heads, 2):
+            columns_of = slice(h * plain_and_turn, (h + 2) * plain_and_turn)
+            two = jnp.dot(normed, query_w[:, columns_of], preferred_element_type=f32)
+            table = turn_ref[...]
+            middle = two[:, NOPE : 2 * NOPE]
+            query_ref[h, :, :NOPE] = two[:, :NOPE].astype(bf16)
+            query_ref[h, :, NOPE:] = rotate(middle, table).astype(bf16)
+            last = two[:, 2 * NOPE :]
+            lane = lax.broadcasted_iota(jnp.int32, last.shape, 1)
+            low, high = pltpu.roll(middle, ROPE, 1), pltpu.roll(last, ROPE, 1)
+            query_ref[h + 1, :, :NOPE] = jnp.where(lane < ROPE, low, high).astype(bf16)
+            query_ref[h + 1, :, NOPE:] = rotate(high, table).astype(bf16)
+
     def expand():
-        @pl.loop(0, experts)
-        def _(e):
-            block = side_block(e)
+        @pl.loop(0, depth)
+        def _(d):
+            block = side_all[pl.ds(2 * d, 2)].reshape(2 * row_count, side_width)
             latent, rest = block[:, :latent_width], block[:, latent_width:]
-            at = pl.ds(pl.multiple_of(e * row_count, row_count), row_count)
+            at = pl.ds(pl.multiple_of(2 * d * row_count, 2 * row_count), 2 * row_count)
             key_block = jnp.dot(latent, key_ref[...], preferred_element_type=f32).astype(bf16)
             value_block = jnp.dot(latent, value_ref[...], preferred_element_type=f32).astype(bf16)
             for h in range(heads):
@@ -442,12 +517,18 @@
             send(heads_ref.at[flip(y, b) * 2 + 1 - core], heads_twin.at[b], heads_sem.at[b], twin)
 
     me = place(z, x, y, core)
-    for target in columns + [x_next, y_next, twin]:
-        give(me, target, True)
+    targets = columns + [x_next, y_next, twin]
+    prepare_rows()
+    for target in targets:
+        pair = copies(me, target, True)
+        pair[0].start()
+        spread.append(pair)
     rows_all[me["ep"], me["tp"]] = row_ref[...]
+    prepare_side()
+    for pair in spread:
+        pair[1].start()
     side_all[me["ep"], me["tp"]] = side_ref[...]
-    for load in loads:
-        load.wait()
+    prepare_queries()
 
     def reduce_after(last):
         for step, back in ((sum_pairs, 0), (sum_relay, 1), (sum_square, 2)):
@@ -462,9 +543,11 @@
         if 0 <= d - 2 < depth:
             forward_corner(d - 2)
         if 0 <= d - 3 < depth:
+            loaded(15)
             expert_plane(d - 3)
         if 0 <= d - 4:
             reduce_after(d - 4)
+    loaded(len(loads))
     expand()
     reduce_after(depth - 1)
     for h in range(heads):
@@ -497,96 +580,65 @@
             copy.wait_send()
 
 
-def layer(rows, side, queries, gain, weights, experts, parts):
-    depth, heads = experts // 2, queries.shape[0]
-    quarter, width = rows.shape
-    row_count = quarter * parts
+def turn_tables(row_count, experts):
+    inverse = rope_base ** (-np.arange(0, ROPE, 2) / ROPE)
+    near, far = np.arange(row_count)[:, None] * inverse, row_count * np.arange(experts)[:, None] * inverse
+
+    def lanes(angle):
+        return np.concatenate([np.cos(angle)] * 2 + [np.sin(angle)] * 2, axis=1).astype(np.float32)
+
+    return lanes(near), lanes(far)
+
+
+def dense_local(
+    mix_in, mix_gain, query_weight, latent_weight, rotary_weight, latent_gain, key_weight,
+    value_weight, output_weight, out_gain, ffn_in, ffn_gain, gate_weight, up_weight, down_weight,
+    routes, route_scores,
+):
+    experts, parts = lax.axis_size("ep"), lax.axis_size("tp")
+    row_count, width = mix_in.shape
+    quarter, depth = row_count // parts, experts // 2
     tokens = experts * row_count
-    vmem, anywhere = pl.BlockSpec(memory_space=pltpu.VMEM), pl.BlockSpec(memory_space=pl.ANY)
+    latent_width = latent_weight.shape[1]
+    heads = query_weight.shape[1] // (NOPE + ROPE)
+    side_width = latent_width + 2 * ROPE
+    base, step = turn_tables(row_count, experts)
+    row = lambda gain: gain.reshape(1, -1)
+    operands = (
+        ffn_in, mix_in, row(ffn_gain), row(mix_gain), row(latent_gain), row(out_gain), routes.T,
+        route_scores.T, jnp.asarray(base), jnp.asarray(step), latent_weight, rotary_weight.T, query_weight,
+        gate_weight[0], up_weight[0], down_weight[0], key_weight, value_weight, output_weight,
+    )
     held = lambda *lead: pltpu.VMEM(lead + (quarter, width), jnp.bfloat16)
     scratch = lambda *shape: pltpu.VMEM(shape, jnp.bfloat16)
     sems = lambda *shape: pltpu.SemaphoreType.DMA(shape)
     gives = depth + 2 + 3 * (depth - 1) + 3 * depth + depth
     return pl.pallas_call(
-        functools.partial(layer_kernel, depth, heads),
+        functools.partial(layer_kernel, depth, heads, side_width),
         out_shape=[jax.ShapeDtypeStruct((quarter, width), jnp.bfloat16)] * 2,
-        in_specs=[vmem] * 4 + [anywhere] * len(weights),
-        out_specs=[vmem] * 2,
+        in_specs=[pl.BlockSpec(memory_space=pl.ANY)] * len(operands),
+        out_specs=[pl.BlockSpec(memory_space=pltpu.VMEM)] * 2,
         scratch_shapes=[
-            held(experts, parts), scratch(experts, parts, quarter, side.shape[1]),
+            held(), scratch(quarter, side_width), scratch(heads, row_count, NOPE + 2 * ROPE),
+            held(experts, parts), scratch(experts, parts, quarter, side_width),
             held(experts, parts), held(depth, 2, 2), held(depth, 2, 2),
             held(depth), held(depth), held(depth), held(depth),
             held(parts), held(), held(2), held(),
-            scratch(heads, tokens, queries.shape[2]), scratch(heads, tokens, VD),
+            scratch(heads, tokens, NOPE + 2 * ROPE), scratch(heads, tokens, VD),
             scratch(row_count, heads * VD), pltpu.VMEM((quarter, width), jnp.float32),
+            pltpu.VMEM((row_count, 2 * ROPE), jnp.float32), pltpu.VMEM((row_count, 2 * ROPE), jnp.float32),
+            pltpu.VMEM((quarter, width), ffn_in.dtype), pltpu.VMEM(mix_in.shape, mix_in.dtype),
         ]
-        + [scratch(*w.shape) for w in weights]
+        + [pltpu.VMEM(a.shape, a.dtype) for a in operands[2:]]
         + [
             sems(2, gives + 1), sems(2, experts, parts), sems(3 + 8 * depth), sems(depth, 2, 2),
-            sems(3, depth), sems(depth), sems(3), sems(len(weights)),
+            sems(3, depth), sems(depth), sems(3), sems(len(operands)),
         ],
         compiler_params=pltpu.CompilerParams(
-            collective_id=0, has_side_effects=True, vmem_limit_bytes=56 * 1024 * 1024
+            collective_id=0, has_side_effects=True, vmem_limit_bytes=60 * 1024 * 1024
         ),
         name="layer",
-    )(rows, side, queries, gain.reshape(1, -1), *weights)
-
-
-def dense_local(
-    mix_in, mix_gain, query_weight, latent_weight, rotary_weight, latent_gain, key_weight,
-    value_weight, output_weight, out_gain, ffn_in, ffn_gain, gate_weight, up_weight, down_weight,
-    routes, route_scores,
-):
-    f32, bf16 = jnp.float32, jnp.bfloat16
-    experts, parts = lax.axis_size("ep"), lax.axis_size("tp")
-    ep, tp = lax.axis_index("ep"), lax.axis_index("tp")
-    row_count, width = mix_in.shape
-    quarter = row_count // parts
-    latent_width = latent_weight.shape[1]
-    half = ROPE // 2
-    first_row = ep * row_count
-
-    def own(array):
-        return lax.dynamic_slice_in_dim(array, tp * quarter, quarter, 0)
-
-    rows = rms_rows(own(ffn_in).astype(f32), ffn_gain).astype(bf16)
-    own_normed = rms_rows(own(mix_in).astype(f32), mix_gain).astype(bf16)
-    latent = rms_rows(jnp.dot(own_normed, latent_weight, preferred_element_type=f32), latent_gain)
-    turned = jnp.dot(own_normed, rotary_weight, preferred_element_type=f32)
-    positions = first_row + jnp.arange(row_count, dtype=jnp.int32)
-    inverse = rope_base ** (-jnp.arange(0, ROPE, 2).astype(f32) / ROPE)
-    angles = positions.astype(f32)[:, None] * inverse[None, :]
-    cosine, sine = jnp.cos(angles), jnp.sin(angles)
-
-    def rotate(vectors, cosine, sine):
-        upper, lower = vectors[..., :half], vectors[..., half:]
-        return jnp.concatenate([upper * cosine - lower * sine, lower * cosine + upper * sine], axis=-1)
-
-    rotary_key = rotate(turned, own(cosine), own(sine))
-    shares = jax.nn.softmax(own(route_scores), axis=-1)
-    named = own(routes)[:, :, None] == jnp.arange(experts, dtype=jnp.int32)[None, None, :]
-    table = jnp.sum(jnp.where(named, shares[:, :, None], 0.0), axis=1)
-    coarse = lax.reduce_precision(table, 8, 7)
-    used = latent_width + ROPE + 2 * experts
-    side_width = -(-used // 128) * 128
-    side = jnp.concatenate(
-        [latent, rotary_key, coarse, table - coarse, jnp.zeros((quarter, side_width - used), f32)],
-        axis=1,
-    ).astype(bf16)
-    normed = rms_rows(mix_in.astype(f32), mix_gain).astype(bf16)
-    head_count = query_weight.shape[1] // (NOPE + ROPE)
-    queries = jnp.dot(normed, query_weight, preferred_element_type=f32).reshape(
-        row_count, head_count, NOPE + ROPE
-    )
-    query_turn = rotate(queries[..., NOPE:], cosine[:, None, :], sine[:, None, :])
-    spare = jnp.zeros((row_count, head_count, side_width - latent_width - ROPE), f32)
-    queries = jnp.concatenate([queries[..., :NOPE], query_turn, spare], axis=-1)
-    queries = queries.astype(bf16).transpose(1, 0, 2)
-    weights = (
-        gate_weight[0], up_weight[0], down_weight[0], key_weight, value_weight, output_weight
-    )
-    mixed, moe_out = layer(rows, side, queries, out_gain, weights, experts, parts)
-    return mixed, moe_out
+    )(*operands)
 
 
 def solution(mesh):

time: 94.9 us -> 72.5 us (0.76)
  other arithmetic: 8.91 us -> 0 us
  matrix products: 6.03 us -> 0 us
  local copies, waits for them, and re-layouts: 8.91 us -> 3.14 us
  Pallas kernels: 69.8 us -> 68.4 us
    dot_general x3 -> x0, matrix products: 6.03 us -> none  [the longest x1 2.41 us: dense_local(): jnp.dot(normed, query_weight, preferred_element_type=f32)]
    unnamed x17 -> x2, local copies, waits for them, and re-layouts: 6.54 us -> 3.14 us
    reduce_sum x4 -> x0, other arithmetic: 3.19 us -> none  [the longest x2 2.38 us: rms_rows(): mean_square = jnp.mean(rows_in * rows_in, axis=-1, keepdims=True)]
    convert_element_type x2 -> x0, other arithmetic: 1.66 us -> none  [the longest x1 1.66 us: dense_local(): rows = rms_rows(own(ffn_in).astype(f32), ffn_gain).astype(bf16)]
    pallas_call x1, Pallas kernels: 69.8 us -> 68.4 us  [dense_local(): pl.pallas_call(functools.partial(layer_kernel, depth, heads, side_width),...]
    another operation x4 -> x0, other arithmetic: 1.22 us -> none
where the time goes in v1:
time: 72.5 us; the launch traced here: 72.2 us
  Pallas kernels  68.4 us (94%)
  local copies, waits for them, and re-layouts  3.14 us (4%)
    pallas_call x1, Pallas kernels, dense_local(): pl.pallas_call(functools.partial(layer_kernel, depth, heads, side_width),...  68.4 us
    unnamed x2, local copies, waits for them, and re-layouts  3.14 us

profile of v1, /device:TPU:0, one launch (start us, length us, event | category | flops | bytes accessed | tf_op | source)
XLA Modules:
  0.0 72.2 jit_solution(11550040602489186448)
XLA Ops:
  0.6 68.4 %layer.1 = (bf16[32,2048]{1,0:T(8,128)(2,1)}, bf16[32,2048]{1,0:T(8,128)(2,1)}) custom-call(bf16[128,2048]{1,0:T(8,128)(2,1)} %ffn_hbm.1, bf16[128,2048]{1,0:T(8,128)(2,1)} %mix_hbm.1, f32[1,2048]{1,0:T(1,128)} %bitcast.14, f32[1,2048]{1,0:T(1,128)} %bitcast.15, f32[1,512]{1,0:T(1,128)} %bitcast.17, f32[1,2048]{1,0:T(1,128)} %bitcast.16, s32[4,128]{1,0:T(4,128)} %bitcast.18, ...), custom_call_target="tpu_custom_call" | custom-call | tf_op jit(solution)/shard_map/layer/pallas_call | solution.py:616
  69.0 1.6 %copy.23 = bf16[32,2048]{1,0:T(8,128)(2,1)} copy(bf16[32,2048]{1,0:T(8,128)(2,1)} %get-tuple-element.4) | data formatting | bytes 262144
  70.6 1.6 %copy.24 = bf16[32,2048]{1,0:T(8,128)(2,1)} copy(bf16[32,2048]{1,0:T(8,128)(2,1)} %get-tuple-element.5) | data formatting | bytes 262144

commit v2 on v1

v2 whole, which is shorter than its diff:
```python
import jax
import jax.numpy as jnp
import functools
import numpy as np
from jax import lax
from jax.experimental import pallas as pl
from jax.experimental.pallas import tpu as pltpu
from jax.sharding import PartitionSpec as P

NOPE = 128
ROPE = 64
VD = 128


norm_eps = 1e-06
clamp_limit = 7.0
gate_slope = 1.702
rope_base = 10000.0


def rms_rows(rows_in, scales):
    mean_square = jnp.mean(rows_in * rows_in, axis=-1, keepdims=True)
    return rows_in * lax.rsqrt(mean_square + norm_eps) * scales


def rms_columns(columns, scales):
    mean_square = jnp.mean(columns * columns, axis=0, keepdims=True)
    return columns * lax.rsqrt(mean_square + norm_eps) * scales[:, None]


def turn_table(positions):
    inverse = rope_base ** (-jnp.arange(0, ROPE, 2).astype(jnp.float32) / ROPE)
    angle_rows = inverse[:, None] * positions.astype(jnp.float32)[None, :]
    return (jnp.cos(angle_rows), jnp.sin(angle_rows))


def clamped_unit(gate_part, linear):
    gate_part = jnp.minimum(gate_part, clamp_limit)
    linear = jnp.clip(linear, -clamp_limit, clamp_limit)
    return gate_part * jax.nn.sigmoid(gate_slope * gate_part) * (linear + 1.0)


def keep_state(running):
    return running


def local(
    mix_in,
    mix_gain,
    query_weight,
    latent_weight,
    rotary_weight,
    latent_gain,
    key_weight,
    value_weight,
    output_weight,
    out_gain,
    ffn_in,
    ffn_gain,
    gate_weight,
    up_weight,
    down_weight,
    routes,
    route_scores,
):
    row_count = mix_in.shape[0]
    first_row = lax.axis_index("ep") * row_count
    last_row = first_row + row_count - 1
    positions = first_row + jnp.arange(row_count, dtype=jnp.int32)
    normed = rms_rows(mix_in.astype(jnp.float32), mix_gain).astype(jnp.bfloat16)
    head_count = query_weight.shape[1] // (NOPE + ROPE)
    half_rope = ROPE // 2
    cosine, sine_rows = turn_table(positions)
    queries = jnp.dot(normed, query_weight, preferred_element_type=jnp.float32).reshape(
        row_count, head_count, NOPE + ROPE
    )
    query_plain = queries[..., :NOPE].astype(jnp.bfloat16)
    query_cos = cosine.T[:, None, :]
    query_sin = sine_rows.T[:, None, :]
    query_upper = queries[..., NOPE : NOPE + half_rope]
    query_lower = queries[..., NOPE + half_rope :]
    query_turn = jnp.concatenate(
        [
            query_upper * query_cos - query_lower * query_sin,
            query_lower * query_cos + query_upper * query_sin,
        ],
        axis=-1,
    ).astype(jnp.bfloat16)
    across = (((0,), (1,)), ((), ()))
    latent = rms_columns(
        lax.dot_general(latent_weight, normed, across, preferred_element_type=jnp.float32),
        latent_gain,
    ).astype(jnp.bfloat16)
    rot_raw = lax.dot_general(rotary_weight, normed, across, preferred_element_type=jnp.float32)
    rotary_key = jnp.concatenate(
        [
            rot_raw[:half_rope] * cosine - rot_raw[half_rope:] * sine_rows,
            rot_raw[half_rope:] * cosine + rot_raw[:half_rope] * sine_rows,
        ],
        axis=0,
    ).astype(jnp.bfloat16)
    score_scale = (NOPE + ROPE) ** (-0.5)
    contract_first = (((0,), (0,)), ((), ()))

    def expand(latent_block):
        key_block = lax.dot_general(
            key_weight, latent_block, contract_first, preferred_element_type=jnp.float32
        ).astype(jnp.bfloat16)
        value_block = lax.dot_general(
            value_weight, latent_block, contract_first, preferred_element_type=jnp.float32
        ).astype(jnp.bfloat16)
        return (key_block, value_block)

    def attend(key_block, value_block, turn_block):
        key_count = key_block.shape[1]
        key_block = key_block.reshape(head_count, NOPE, key_count)
        value_block = value_block.reshape(head_count, VD, key_count)
        scores = jnp.einsum(
            "ihd,hdj->hij", query_plain, key_block, preferred_element_type=jnp.float32
        )
        scores = scores + jnp.einsum(
            "ihd,dj->hij", query_turn, turn_block, preferred_element_type=jnp.float32
        )
        key_places = jnp.arange(key_count, dtype=jnp.int32)
        allowed = key_places[None, :] <= positions[:, None]
        weights = jnp.where(allowed[None], jnp.exp(scores * score_scale), 0.0)
        weighted = jnp.einsum(
            "hij,hdj->hid",
            weights.astype(jnp.bfloat16),
            value_block,
            preferred_element_type=jnp.float32,
        )
        return (jnp.sum(weights, axis=-1), weighted)

    initial = (
        jnp.zeros((head_count, row_count), jnp.float32),
        jnp.zeros((head_count, row_count, VD), jnp.float32),
    )
    shard_piece = (
        lax.all_gather(latent, "ep", axis=1, tiled=True),
        lax.all_gather(rotary_key, "ep", axis=1, tiled=True),
    )

    def compute_piece(running):
        key_block, value_block = expand(shard_piece[0])
        return attend(key_block, value_block, shard_piece[1])

    totals, weighted = lax.cond(jnp.int32(0) > last_row, keep_state, compute_piece, initial)
    attended = (weighted / totals[..., None]).astype(jnp.bfloat16)
    mixing = output_weight.reshape(head_count, VD, output_weight.shape[1])
    partial_value = jnp.einsum("hid,hde->ie", attended, mixing, preferred_element_type=jnp.float32)
    projected = lax.psum_scatter(
        lax.optimization_barrier(partial_value.astype(jnp.bfloat16))
        .astype(jnp.float32)
        .astype(jnp.bfloat16),
        "tp",
        scatter_dimension=0,
        tiled=True,
    ).astype(jnp.float32)
    mixed = rms_rows(projected, out_gain).astype(jnp.bfloat16)
    tokens = ffn_in.shape[0]
    part_count = lax.axis_size("tp")
    quarter_rows = tokens // part_count
    experts = lax.axis_size("ep")
    choose = routes.shape[1]
    capacity = max(2, 2 * quarter_rows * choose // experts)
    slot_count = capacity * part_count
    tp_index = lax.axis_index("tp")
    normed_b = rms_rows(ffn_in.astype(jnp.float32), ffn_gain).astype(jnp.bfloat16)
    padded = jnp.concatenate([normed_b, jnp.zeros((1, normed_b.shape[1]), jnp.bfloat16)], axis=0)
    gate_share = jax.nn.softmax(route_scores, axis=-1)
    grouped = routes.reshape(part_count, quarter_rows * choose)
    onehot = (grouped[:, :, None] == jnp.arange(experts, dtype=jnp.int32)[None, None, :]).astype(
        jnp.int32
    )
    slot_rank = jnp.sum((jnp.cumsum(onehot, axis=1) - 1) * onehot, axis=2)
    slot_index = jnp.arange(part_count, dtype=jnp.int32)[:, None] * capacity + slot_rank
    place_index = (slot_index * experts + grouped).reshape(-1)
    owners = jnp.arange(tokens * choose, dtype=jnp.int32) // choose
    slot_token = jnp.full((slot_count * experts,), tokens, jnp.int32).at[place_index].set(owners)
    unit_count = gate_weight.shape[2]
    chosen = lax.dynamic_slice_in_dim(
        slot_token, tp_index * capacity * experts, capacity * experts, 0
    )
    outgoing = padded[chosen].reshape(capacity, experts, -1)
    arrived = lax.all_to_all(outgoing, "ep", split_axis=1, concat_axis=1, tiled=True)
    row_block = lax.all_gather(arrived, "tp", axis=0, tiled=True)
    block_slots = row_block.shape[0]
    flat_rows = row_block.reshape(-1, row_block.shape[2])
    gate_part = jnp.dot(flat_rows, gate_weight[0], preferred_element_type=jnp.float32)
    up_part = jnp.dot(flat_rows, up_weight[0], preferred_element_type=jnp.float32)
    hidden = (
        clamped_unit(gate_part, up_part).astype(jnp.bfloat16).reshape(block_slots, -1, unit_count)
    )
    sources = hidden.shape[1]
    hidden_flat = hidden.reshape(slot_count * sources, unit_count)
    partial_value = jnp.dot(hidden_flat, down_weight[0], preferred_element_type=jnp.float32)
    result = lax.psum_scatter(
        lax.optimization_barrier(partial_value.astype(jnp.bfloat16))
        .astype(jnp.float32)
        .astype(jnp.bfloat16),
        "tp",
        scatter_dimension=0,
        tiled=True,
    )
    result = result.reshape(capacity, sources, -1)
    returned = lax.all_to_all(result, "ep", split_axis=1, concat_axis=1, tiled=True)
    back_rows = returned.reshape(capacity * experts, -1)
    own_rank = lax.dynamic_index_in_dim(slot_rank, tp_index, 0, keepdims=False)
    own_expert = lax.dynamic_index_in_dim(grouped, tp_index, 0, keepdims=False)
    picked = (
        back_rows[own_rank * experts + own_expert]
        .astype(jnp.float32)
        .reshape(quarter_rows, choose, -1)
    )
    own_gates = lax.dynamic_slice_in_dim(gate_share, tp_index * quarter_rows, quarter_rows, 0)
    moe_out = jnp.sum(picked * own_gates[:, :, None], axis=1).astype(jnp.bfloat16)
    return (mixed, moe_out)


MESH = pl.DeviceIdType.MESH
PIECES = 2
OUTER = (
    ["prep", "lats", "Lown", "Y0b"],
    ["X0a", "XY0", "Z10", "Z11"],
    ["C00", "qry", "Z20", "LZ1"],
    ["C01", "LX0", "E0", "Z21"],
    ["P0a", "Y1", "LY0", "D10"],
    ["Z30", "LZ2", "X1", "D11"],
    ["LC0", "E1", "Z31", "LY1"],
    ["P1a", "D20", "X2", "Y2"],
    ["P0b", "D21", "R00", "E2"],
    ["LX2", "P1b", "P2a", "D30"],
    ["LZ3", "Y3", "LY2", "X3"],
    ["P2b", "LD1", "D31", "A0"],
    ["LD2", "LX1", "R20", "E3"],
    ["R10", "LD3", "R21", "LY3"],
    ["P3a", "R11", "Q20", "A2"],
    ["Q21", "LX3", "A1", "Q10"],
    ["P3b", "R30", "R01", "A3"],
    ["R31", "PR", "Q00", "Q11"],
    ["Q30", "CH", "Q31", "Q01"],
    ["FH", "FM"],
)
INNER = (
    ["prep", "lats", "Lown", "Y0b"],
    ["X0a", "Z10", "Z20", "Z11"],
    ["XY0", "Z21", "LZ2", "C00"],
    ["LZ1", "LX0", "Z30", "C01"],
    ["LY0", "E0", "D10", "Z31"],
    ["Y1", "D20", "D11", "X1"],
    ["LY2", "LX2", "Y2", "X2"],
    ["P0a", "D21", "LZ3", "LC0"],
    ["D30", "E1", "LY1", "E2"],
    ["P1a", "P2a", "P2b", "LY3"],
    ["LD1", "P1b", "D31", "X3"],
    ["qry", "R10", "Y3", "A0"],
    ["LD2", "R20", "E3", "LD3"],
    ["LX3", "R21", "R11", "P0b"],
    ["A2", "P3a", "LX1", "Q20"],
    ["Q21", "P3b", "A3", "A1"],
    ["R30", "Q10", "R31", "PR"],
    ["R00", "R01", "Q11", "Q30"],
    ["CH", "Q31", "Q00", "Q01"],
    ["FM", "FH"],
)


def flip(value, bits):
    bit = 1
    while bit <= bits:
        if bits & bit:
            value = value + bit - 2 * bit * ((value // bit) % 2)
        bit *= 2
    return value


def here():
    ep, tp = lax.axis_index("ep"), lax.axis_index("tp")
    return ep // 2, ep % 2, tp // 2, tp % 2


def place(z, x, y, core):
    return {"ep": z * 2 + x, "tp": y * 2 + core}


def greet(partners):
    barrier = pltpu.get_barrier_semaphore()
    for partner in partners:
        pl.semaphore_signal(barrier, inc=1, device_id=partner, device_id_type=MESH)
    pl.semaphore_wait(barrier, len(partners))


def layer_kernel(
    width, heads,
    ffn_hbm, mix_hbm, ffn_gain_hbm, mix_gain_hbm, latent_gain_hbm, out_gain_hbm, routes_hbm, scores_hbm,
    base_hbm, step_hbm, latent_hbm, rotary_hbm, query_hbm, gate_hbm, up_hbm, down_hbm, key_hbm,
    value_hbm, output_hbm, mixed_ref, moe_ref,
    rows_all, lat_all, part_ref, work, twin_in, hop_in, direct_in, relay_in, column_in,
    heads_ref, heads_work, heads_twin, heads_in, query_ref, keys, values, weighted, totals, attended, own_total,
    table_ref, turn_ref, ffn_ref, mix_ref,
    ffn_gain, mix_gain, latent_gain, gain_ref, routes_ref, scores_ref, base_ref, step_ref, latent_ref,
    rotary_ref, query_w, gate_ref, up_ref, down_ref, key_ref, value_ref, output_ref,
    row_send, row_recv, lat_send, lat_recv, send_sem, twin_sem, square_sem, column_sem, heads_sem, load_sem,
):
    f32, bf16 = jnp.float32, jnp.bfloat16
    ep, tp = lax.axis_index("ep"), lax.axis_index("tp")
    z, x, y, core = here()
    inner = ((z + 1) // 2) % 2
    planes = [z, flip(z, 1)]
    far = flip(z, 2)
    planes.append(far + inner * (1 - 2 * (far % 2)))
    planes.append(flip(planes[2], 1))
    depth = len(planes)
    x_next, y_next, twin = place(z, 1 - x, y, core), place(z, x, 1 - y, core), place(z, x, y, 1 - core)
    z_out, z_in = place(planes[1], x, y, core), place(flip(z, 3), x, y, core)
    parts, quarter = part_ref.shape[2:4]
    row_count = parts * quarter
    block_rows = 2 * row_count
    experts = 2 * depth
    half = ROPE // 2
    piece = quarter // PIECES
    first_own = pl.multiple_of(tp * quarter, quarter)
    copied = (
        (ffn_hbm.at[pl.ds(first_own, quarter)], ffn_ref), (ffn_gain_hbm, ffn_gain),
        (mix_hbm, mix_ref), (mix_gain_hbm, mix_gain), (rotary_hbm, rotary_ref),
        (base_hbm, base_ref), (step_hbm, step_ref), (routes_hbm, routes_ref), (scores_hbm, scores_ref),
        (latent_hbm, latent_ref), (latent_gain_hbm, latent_gain), (query_hbm, query_w),
        (gate_hbm, gate_ref), (up_hbm, up_ref), (down_hbm, down_ref),
        (key_hbm, key_ref), (value_hbm, value_ref), (output_hbm, output_ref), (out_gain_hbm, gain_ref),
    )
    loads = [pltpu.make_async_copy(src, dst, load_sem.at[n]) for n, (src, dst) in enumerate(copied)]
    for load in loads:
        load.start()
    waited = [0]

    def loaded(count):
        while waited[0] < count:
            loads[waited[0]].wait()
            waited[0] += 1

    greet([place(p, x, y, core) for p in planes[1:]] + [x_next, y_next, twin])
    always = None
    issued = {}

    def guarded(condition, action):
        if condition is None:
            action()
        else:
            pl.when(condition)(action)

    role = ["both"]

    def post(key, build, condition=always):
        if condition == "inner":
            if role[0] == "outer":
                return
            condition = always if role[0] == "inner" else is_inner
        issued.setdefault(key, (build, condition))
        guarded(condition, lambda: build().start())

    numbers = {}

    def number(kind, key):
        taken = numbers.setdefault(kind, {})
        return taken.setdefault(key, len(taken))

    def at_piece(ref, g):
        return ref if g is None else ref.at[pl.ds(g * piece, piece)]

    def row_copy(origin, g, target, key):
        e, t = origin["ep"], origin["tp"]
        ref = at_piece(rows_all.at[e, t], g)
        return pltpu.make_async_remote_copy(
            src_ref=ref, dst_ref=ref, send_sem=row_send.at[number("row", key)],
            recv_sem=row_recv.at[e, t, g or 0], device_id=target, device_id_type=MESH,
        )

    def give_row(name, origin, g, target, towards, condition=always):
        key = (name, g, towards)
        post(("row",) + key, lambda: row_copy(origin, g, target, key), condition)

    def take_row(origin, g):
        row_copy(origin, g, twin, ("any",)).wait_recv()

    def lat_copy(origin, target, key):
        e, t = origin["ep"], origin["tp"]
        ref = lat_all.at[e, t]
        return pltpu.make_async_remote_copy(
            src_ref=ref, dst_ref=ref, send_sem=lat_send.at[number("lat", key)],
            recv_sem=lat_recv.at[e, t], device_id=target, device_id_type=MESH,
        )

    def give_lat(name, origin, target, towards, condition=always):
        key = (name, towards)
        post(("lat",) + key, lambda: lat_copy(origin, target, key), condition)

    def take_lat(origin):
        lat_copy(origin, twin, ("any",)).wait_recv()

    def make(src, dst, sem, target, key):
        return pltpu.make_async_remote_copy(
            src_ref=src, dst_ref=dst, send_sem=send_sem.at[number("sum", key)], recv_sem=sem,
            device_id=target, device_id_type=MESH,
        )

    def send(src, dst, sem, target, *key):
        post(("sum",) + key, lambda: make(src, dst, sem, target, key))

    def arrive(dst, sem):
        make(dst, dst, sem, twin, ("any",)).wait_recv()

    is_inner, is_outer = inner == 1, inner == 0
    up_out, up_in = z % 2 == 0, z == 1
    me = place(z, x, y, core)

    origins = {
        (s, dx, dy): place(planes[s], flip(x, dx), flip(y, dy), core)
        for s in range(depth) for dx in (0, 1) for dy in (0, 1)
    }

    def origin_of(s, dx, dy):
        return origins[s, dx, dy]

    def own_rows():
        for g in range(PIECES):
            give_row("own", me, g, z_out, "out")
            give_row("own", me, g, z_in, "in", "inner")
            give_row("own", me, g, x_next, "x")
            give_row("own", me, PIECES - 1 - g, y_next, "y")
        give_row("own", me, None, twin, "twin")

    def side_rows(first):
        by_x, by_y = origin_of(0, 1, 0), origin_of(0, 0, 1)
        for g in range(PIECES // 2):
            if first == "x":
                take_row(by_x, g)
                give_row("x0", by_x, g, y_next, "y")
            else:
                take_row(by_y, PIECES - 1 - g)
                give_row("y0", by_y, PIECES - 1 - g, x_next, "x")

    def side_rows_rest():
        by_x, by_y = origin_of(0, 1, 0), origin_of(0, 0, 1)
        for g in range(PIECES // 2):
            take_row(by_x, PIECES - 1 - g)
            take_row(by_y, g)
        give_row("x0", by_x, None, twin, "twin")
        give_row("y0", by_y, None, twin, "twin")

    def last(g):
        return g == PIECES - 1

    def corner_rows(g):
        corner = origin_of(0, 1, 1)
        take_row(corner, g)
        give_row("c0", corner, g, z_out, "out")
        give_row("c0", corner, g, z_in, "in", "inner")
        if last(g):
            give_row("c0", corner, None, twin, "twin")

    def column_rows(s, g, dx):
        origin = origin_of(s, dx, dx)
        name = f"{'zd'[dx]}{s}"
        take_row(origin, g)
        if s == 1:
            give_row(name, origin, g, z_in, "in", "inner")
        else:
            give_row(name, origin, g, z_out, "out", "inner")
        if not dx:
            give_row(name, origin, g, x_next, "x")
            give_row(name, origin, g, y_next, "y")
        if last(g):
            give_row(name, origin, None, twin, "twin")

    def square_rows(s, dx):
        origin = origin_of(s, dx, 1 - dx)
        for g in range(PIECES):
            take_row(origin, g)
        give_row(f"{'yx'[dx]}{s}", origin, None, twin, "twin")

    def own_lats():
        give_lat("own", me, z_out, "out", up_out)
        give_lat("own", me, z_in, "in", up_in)
        give_lat("own", me, x_next, "x")
        give_lat("own", me, y_next, "y")
        give_lat("own", me, twin, "twin")

    def side_lats(dx):
        origin = origin_of(0, dx, 1 - dx)
        name = f"{'yx'[dx]}0"
        take_lat(origin)
        if dx:
            give_lat(name, origin, y_next, "y")
        give_lat(name, origin, twin, "twin")

    def corner_lats():
        corner = origin_of(0, 1, 1)
        take_lat(corner)
        give_lat("c0", corner, z_out, "out", up_out)
        give_lat("c0", corner, z_in, "in", up_in)
        give_lat("c0", corner, twin, "twin")

    lower = [plane < z for plane in planes]
    up_two = z == 2

    def below(s):
        return lower[s]

    def column_lats(s, dx):
        origin = origin_of(s, dx, dx)
        name = f"{'zd'[dx]}{s}"

        @pl.when(below(s))
        def _():
            take_lat(origin)

        if s == 1:
            give_lat(name, origin, z_in, "in", up_in)
        else:
            give_lat(name, origin, z_out, "out", up_two)
        if not dx:
            give_lat(name, origin, x_next, "x", below(s))
            give_lat(name, origin, y_next, "y", below(s))
        give_lat(name, origin, twin, "twin", below(s))

    def square_lats(s, dx):
        origin = origin_of(s, dx, 1 - dx)

        @pl.when(below(s))
        def _():
            take_lat(origin)

        give_lat(f"{'yx'[dx]}{s}", origin, twin, "twin", below(s))

    def expert_plane(s):
        loaded(15)
        for a in (0, 1):
            for b in (0, 1):
                take_row(place(planes[s], flip(x, a), flip(y, b), 1 - core), None)
        pair = pl.ds(planes[s] * 2, 2)
        block = rows_all[pair, :, :, :width].reshape(block_rows, width)
        gate_part = jnp.dot(block, gate_ref[...], preferred_element_type=f32)
        up_part = jnp.dot(block, up_ref[...], preferred_element_type=f32)
        hidden = clamped_unit(gate_part, up_part).astype(bf16)
        table = rows_all[pair, :, :, width:].reshape(block_rows, 2 * ROPE)
        lane = lax.broadcasted_iota(jnp.int32, table.shape, 1)
        is_mine = (lane == ROPE + ep) | (lane == ROPE + experts + ep)
        share = jnp.sum(jnp.where(is_mine, table.astype(f32), 0.0), axis=1, keepdims=True)
        chunk = 512
        for n in range(0, width, chunk):
            out = jnp.dot(hidden, down_ref[:, n : n + chunk], preferred_element_type=f32) * share
            part_ref[s, :, :, :, n : n + chunk] = out.astype(bf16).reshape(2, parts, quarter, chunk)
        for a, b in ((1, 1), (0, 1), (1, 0), (0, 0)) if s % 2 else ((1, 1), (1, 0), (0, 1), (0, 0)):
            mine = part_ref.at[s, flip(x, a), flip(y, b) * 2 + 1 - core]
            send(mine, twin_in.at[s, a, b], twin_sem.at[s, a, b], twin, "twin", s, a, b)

    def paired(s, a, b, g=None):
        if not g:
            arrive(twin_in.at[s, a, b], twin_sem.at[s, a, b])
        rows = slice(None) if g is None else rows_of(g)
        own = part_ref[s, flip(x, a), flip(y, b) * 2 + core, rows]
        return own.astype(f32) + twin_in[s, a, b, rows].astype(f32)

    def rows_of(g):
        return pl.ds(g * piece, piece)

    def sum_pairs(s, corner):
        a, b = (1, 1) if corner else (0, 1) if s % 2 else (1, 0)
        landing, which = (hop_in, 0) if corner else (direct_in, 1)
        work[s, a, b] = paired(s, a, b).astype(bf16)
        for g in range(PIECES):
            send(
                work.at[s, a, b, rows_of(g)], landing.at[s, rows_of(g)], square_sem.at[which, s, g],
                y_next if s % 2 else x_next, which, s, g,
            )

    def sum_relay(s, g):
        a, b = (1, 0) if s % 2 else (0, 1)
        rows = rows_of(g)
        value = paired(s, a, b, g)
        arrive(hop_in.at[s, rows], square_sem.at[0, s, g])
        work[s, a, b, rows] = (value + hop_in[s, rows].astype(f32)).astype(bf16)
        send(
            work.at[s, a, b, rows], relay_in.at[s, rows], square_sem.at[2, s, g],
            x_next if s % 2 else y_next, 2, s, g,
        )

    def sum_square(s, g):
        rows = rows_of(g)
        value = paired(s, 0, 0, g)
        arrive(direct_in.at[s, rows], square_sem.at[1, s, g])
        value = value + direct_in[s, rows].astype(f32)
        arrive(relay_in.at[s, rows], square_sem.at[2, s, g])
        value = value + relay_in[s, rows].astype(f32)
        if s:
            work[s, 0, 0, rows] = value.astype(bf16)
            send(
                work.at[s, 0, 0, rows], column_in.at[z, rows], column_sem.at[z, g],
                place(planes[s], x, y, core), "column", s, g,
            )
        else:
            own_total[rows, :] = value

    across = (((1,), (1,)), ((), ()))
    score_scale = (NOPE + ROPE) ** (-0.5)

    def angles():
        near = base_ref[...]
        swapped = pltpu.roll(near, ROPE, 1)
        lane = lax.broadcasted_iota(jnp.int32, near.shape, 1)
        cosine, sine = jnp.where(lane < ROPE, near, swapped), jnp.where(lane < ROPE, swapped, near)
        step = jnp.broadcast_to(step_ref[pl.ds(ep, 1), :], near.shape)
        step_swapped = pltpu.roll(step, ROPE, 1)
        step_cos, step_sin = jnp.where(lane < ROPE, step, step_swapped), jnp.where(lane < ROPE, step_swapped, step)
        turn_ref[...] = jnp.where(
            lane < ROPE, cosine * step_cos - sine * step_sin, sine * step_cos + cosine * step_sin
        )

    def rotate(vectors, table):
        lane = lax.broadcasted_iota(jnp.int32, vectors.shape, 1)
        size = vectors.shape[1]
        turned = jnp.where(
            lane < half, -pltpu.roll(vectors, size - half, 1), pltpu.roll(vectors, half, 1)
        )
        sine = pltpu.roll(table, size - ROPE, 1)
        return jnp.where(lane < ROPE, vectors * table + turned * sine, 0.0)

    own = pl.ds(first_own, quarter)

    def own_normed():
        return rms_rows(mix_ref[own, :].astype(f32), mix_gain[...]).astype(bf16)

    def prepare_rows():
        loaded(9)
        rows_all[ep, tp, :, :width] = rms_rows(ffn_ref[...].astype(f32), ffn_gain[...]).astype(bf16)
        angles()
        turned = lax.dot_general(own_normed(), rotary_ref[...], across, preferred_element_type=f32)
        turned = jnp.concatenate([turned, jnp.zeros((quarter, ROPE), f32)], axis=1)
        rotary_key = rotate(turned, turn_ref[own, :])
        scores = scores_ref[...]
        shares = jnp.exp(scores - jnp.max(scores, axis=0, keepdims=True))
        shares = shares / jnp.sum(shares, axis=0, keepdims=True)
        routes = routes_ref[...]
        lane = lax.broadcasted_iota(jnp.int32, (2 * ROPE, row_count), 0)
        named = jnp.zeros((2 * ROPE, row_count), f32)
        for k in range(routes.shape[0]):
            hit = (lane == routes[k : k + 1] + ROPE) | (lane == routes[k : k + 1] + ROPE + experts)
            named = named + jnp.where(hit, shares[k : k + 1], 0.0)
        coarse = named.astype(bf16).astype(f32)
        table_ref[...] = jnp.where(lane < ROPE + experts, coarse, named - coarse).T
        rows_all[ep, tp, :, width:] = (rotary_key + table_ref[own, :]).astype(bf16)

    def prepare_lats():
        loaded(11)
        latent = jnp.dot(own_normed(), latent_ref[...], preferred_element_type=f32)
        lat_all[ep, tp] = rms_rows(latent, latent_gain[...]).astype(bf16)

    def prepare_queries():
        loaded(12)
        normed = rms_rows(mix_ref[...].astype(f32), mix_gain[...]).astype(bf16)
        for h in range(0, heads, 2):
            columns_of = slice(h * (NOPE + ROPE), (h + 2) * (NOPE + ROPE))
            two = jnp.dot(normed, query_w[:, columns_of], preferred_element_type=f32)
            table = turn_ref[...]
            middle, last = two[:, NOPE : 2 * NOPE], two[:, 2 * NOPE :]
            lane = lax.broadcasted_iota(jnp.int32, last.shape, 1)
            low, high = pltpu.roll(middle, ROPE, 1), pltpu.roll(last, ROPE, 1)
            query_ref[h, :, :NOPE] = two[:, :NOPE].astype(bf16)
            query_ref[h, :, NOPE:] = rotate(middle, table).astype(bf16)
            query_ref[h + 1, :, :NOPE] = jnp.where(lane < ROPE, low, high).astype(bf16)
            query_ref[h + 1, :, NOPE:] = rotate(high, table).astype(bf16)

    def attend_block(s):
        for a in (0, 1):
            for b in (0, 1):
                take_lat(place(planes[s], flip(x, a), flip(y, b), 1 - core))
        pair = pl.ds(planes[s] * 2, 2)
        latent = lat_all[pair].reshape(block_rows, lat_all.shape[3])
        rest = rows_all[pair, :, :, width:].reshape(block_rows, 2 * ROPE)
        key_block = jnp.dot(latent, key_ref[...], preferred_element_type=f32).astype(bf16)
        value_block = jnp.dot(latent, value_ref[...], preferred_element_type=f32).astype(bf16)
        for h in range(heads):
            keys[h, :, :NOPE] = key_block[:, h * NOPE : (h + 1) * NOPE]
            keys[h, :, NOPE:] = rest
            values[h] = value_block[:, h * VD : (h + 1) * VD]
        shape = (row_count, block_rows)
        places = lax.broadcasted_iota(jnp.int32, shape, 0) + ep * row_count
        allowed = lax.broadcasted_iota(jnp.int32, shape, 1) + planes[s] * block_rows <= places
        for h in range(heads):
            scores = lax.dot_general(query_ref[h], keys[h], across, preferred_element_type=f32)
            weights = jnp.where(allowed, jnp.exp(scores * score_scale), 0.0)
            total = jnp.broadcast_to(jnp.sum(weights, axis=1, keepdims=True), (row_count, VD))
            update = jnp.dot(weights.astype(bf16), values[h], preferred_element_type=f32)
            totals[h] = total if s == 0 else totals[h] + total
            weighted[h] = update if s == 0 else weighted[h] + update

    def attend_plane(s):
        loaded(17)
        if s == 0:
            attend_block(s)
        else:
            pl.when(below(s))(lambda: attend_block(s))

    def project():
        loaded(18)
        for h in range(heads):
            attended[:, h * VD : (h + 1) * VD] = (weighted[h] / totals[h]).astype(bf16)
        chunk = 512
        for n in range(0, width, chunk):
            out = jnp.dot(attended[...], output_ref[:, n : n + chunk], preferred_element_type=f32)
            heads_ref[:, :, n : n + chunk] = out.astype(bf16).reshape(parts, quarter, chunk)
        for b in (1, 0):
            send(
                heads_ref.at[flip(y, b) * 2 + 1 - core], heads_twin.at[b], heads_sem.at[b], twin,
                "heads", b,
            )

    def cross_heads():
        arrive(heads_twin.at[1], heads_sem.at[1])
        heads_work[...] = (
            heads_ref[(1 - y) * 2 + core].astype(f32) + heads_twin[1].astype(f32)
        ).astype(bf16)
        send(heads_work, heads_in, heads_sem.at[2], y_next, "heads", 2)

    def finish_heads():
        loaded(len(loads))
        arrive(heads_twin.at[0], heads_sem.at[0])
        arrive(heads_in, heads_sem.at[2])
        projected = (
            heads_ref[y * 2 + core].astype(f32) + heads_twin[0].astype(f32) + heads_in[...].astype(f32)
        )
        mixed_ref[...] = rms_rows(projected, gain_ref[...]).astype(bf16)

    def finish_moe():
        for g in range(PIECES):
            rows = rows_of(g)
            total = own_total[rows, :]
            for s in range(1, depth):
                arrive(column_in.at[planes[s], rows], column_sem.at[planes[s], g])
                total = total + column_in[planes[s], rows].astype(f32)
            moe_ref[rows, :] = total.astype(bf16)

    def start_rows():
        prepare_rows()
        own_rows()

    steps = {
        "prep": start_rows, "lats": prepare_lats, "qry": prepare_queries, "Lown": own_lats,
        "X0a": lambda: side_rows("x"), "Y0b": lambda: side_rows("y"), "XY0": side_rows_rest,
        "C00": lambda: corner_rows(0), "C01": lambda: corner_rows(1),
        "LX0": lambda: side_lats(1), "LY0": lambda: side_lats(0), "LC0": corner_lats,
        "PR": project, "CH": cross_heads, "FH": finish_heads, "FM": finish_moe,
    }
    kinds = {
        "Z": lambda s, g: column_rows(s, g, 0), "D": lambda s, g: column_rows(s, g, 1),
        "X": lambda s: square_rows(s, 1), "Y": lambda s: square_rows(s, 0),
        "LZ": lambda s: column_lats(s, 0), "LD": lambda s: column_lats(s, 1),
        "LX": lambda s: square_lats(s, 1), "LY": lambda s: square_lats(s, 0),
        "E": expert_plane, "A": attend_plane, "R": sum_relay, "Q": sum_square,
    }

    def run(step):
        if step in steps:
            steps[step]()
        elif step[0] == "P":
            sum_pairs(int(step[1]), step[2] == "a")
        else:
            kind = step.rstrip("0123456789")
            kinds[kind](*(int(digit) for digit in step[len(kind) :]))

    orders = [sum(order, []) for order in (OUTER, INNER)]
    shared = 0
    while orders[0][shared] == orders[1][shared]:
        run(orders[0][shared])
        shared += 1
    ready, sent = waited[0], dict(issued)
    for name, chosen, order in (("outer", is_outer, orders[0]), ("inner", is_inner, orders[1])):
        role[0], waited[0] = name, ready
        issued.clear()
        issued.update(sent)

        @pl.when(chosen)
        def _():
            for step in order[shared:]:
                run(step)
            for build, condition in issued.values():
                guarded(condition, lambda: build().wait_send())


def turn_tables(row_count, experts):
    inverse = rope_base ** (-np.arange(0, ROPE, 2) / ROPE)
    near, far = np.arange(row_count)[:, None] * inverse, row_count * np.arange(experts)[:, None] * inverse

    def lanes(angle):
        return np.concatenate([np.cos(angle)] * 2 + [np.sin(angle)] * 2, axis=1).astype(np.float32)

    return lanes(near), lanes(far)


def dense_local(
    mix_in, mix_gain, query_weight, latent_weight, rotary_weight, latent_gain, key_weight,
    value_weight, output_weight, out_gain, ffn_in, ffn_gain, gate_weight, up_weight, down_weight,
    routes, route_scores,
):
    experts, parts = lax.axis_size("ep"), lax.axis_size("tp")
    row_count, width = mix_in.shape
    quarter, depth = row_count // parts, experts // 2
    block_rows = 2 * row_count
    heads = query_weight.shape[1] // (NOPE + ROPE)
    base, step = turn_tables(row_count, experts)
    row = lambda gain: gain.reshape(1, -1)
    operands = (
        ffn_in, mix_in, row(ffn_gain), row(mix_gain), row(latent_gain), row(out_gain), routes.T,
        route_scores.T, jnp.asarray(base), jnp.asarray(step), latent_weight, rotary_weight.T, query_weight,
        gate_weight[0], up_weight[0], down_weight[0], key_weight, value_weight, output_weight,
    )
    held = lambda *lead: pltpu.VMEM(lead + (quarter, width), jnp.bfloat16)
    scratch = lambda *shape: pltpu.VMEM(shape, jnp.bfloat16)
    wide = lambda *shape: pltpu.VMEM(shape, jnp.float32)
    sems = lambda *shape: pltpu.SemaphoreType.DMA(shape)
    return pl.pallas_call(
        functools.partial(layer_kernel, width, heads),
        out_shape=[pltpu.VMEM((quarter, width), jnp.bfloat16)] * 2,
        in_specs=[pl.BlockSpec(memory_space=pl.ANY)] * len(operands),
        out_specs=[pl.BlockSpec(memory_space=pltpu.VMEM)] * 2,
        scratch_shapes=[
            scratch(experts, parts, quarter, width + 2 * ROPE),
            scratch(experts, parts, quarter, latent_weight.shape[1]),
            held(depth, 2, parts), held(depth, 2, 2), held(depth, 2, 2),
            held(depth), held(depth), held(depth), held(depth),
            held(parts), held(), held(2), held(),
            scratch(heads, row_count, NOPE + 2 * ROPE), scratch(heads, block_rows, NOPE + 2 * ROPE),
            scratch(heads, block_rows, VD), wide(heads, row_count, VD), wide(heads, row_count, VD),
            scratch(row_count, heads * VD), wide(quarter, width),
            wide(row_count, 2 * ROPE), wide(row_count, 2 * ROPE),
            pltpu.VMEM((quarter, width), ffn_in.dtype), pltpu.VMEM(mix_in.shape, mix_in.dtype),
        ]
        + [pltpu.VMEM(a.shape, a.dtype) for a in operands[2:]]
        + [
            sems(96), sems(experts, parts, PIECES), sems(48), sems(experts, parts), sems(64),
            sems(depth, 2, 2), sems(3, depth, PIECES), sems(depth, PIECES), sems(3), sems(len(operands)),
        ],
        compiler_params=pltpu.CompilerParams(
            collective_id=0, has_side_effects=True, vmem_limit_bytes=60 * 1024 * 1024
        ),
        name="layer",
    )(*operands)


def solution(mesh):
    experts, parts = mesh.shape["ep"], mesh.shape["tp"]

    def body(*args):
        quarter, choose = args[10].shape[0] // parts, args[15].shape[1]
        every_row = 2 * quarter * choose >= quarter * experts
        paired = parts == 4 and experts == 8 and quarter % (16 * PIECES) == 0
        return (dense_local if every_row and paired else local)(*args)
    placed = (
        P("ep", None),
        P(),
        P(None, "tp"),
        P(),
        P(),
        P(),
        P(None, "tp"),
        P(None, "tp"),
        P("tp", None),
        P(),
        P("ep", None),
        P(),
        P("ep", None, "tp"),
        P("ep", None, "tp"),
        P("ep", "tp", None),
        P("ep", None),
        P("ep", None),
    )
    return jax.shard_map(
        body,
        mesh=mesh,
        in_specs=placed,
        out_specs=(P(("ep", "tp"), None), P(("ep", "tp"), None)),
        check_vma=False,
    )
```

time: 72.5 us -> 53 us (0.73)
  Pallas kernels: 68.4 us -> 50.9 us
  local copies, waits for them, and re-layouts: 3.14 us -> 1.31 us
    pallas_call x1, Pallas kernels: 68.4 us -> 50.9 us  [dense_local(): pl.pallas_call(functools.partial(layer_kernel, width, heads), out_shape=[...]
    unnamed x2, local copies, waits for them, and re-layouts: 3.14 us -> 1.31 us
where the time goes in v2:
time: 53 us; the launch traced here: 52.8 us
  Pallas kernels  50.9 us (96%)
  local copies, waits for them, and re-layouts  1.31 us (2%)
  between operations  0.65 us (1%)
    pallas_call x1, Pallas kernels, dense_local(): pl.pallas_call(functools.partial(layer_kernel, width, heads), out_shape=[...  50.9 us
    unnamed x2, local copies, waits for them, and re-layouts  1.31 us

profile of v2, /device:TPU:0, one launch (start us, length us, event | category | flops | bytes accessed | tf_op | source)
XLA Modules:
  0.0 52.8 jit_solution(13415300581321319219)
XLA Ops:
  0.6 50.9 %layer.1 = (bf16[32,2048]{1,0:T(8,128)(2,1)S(1)}, bf16[32,2048]{1,0:T(8,128)(2,1)S(1)}) custom-call(bf16[128,2048]{1,0:T(8,128)(2,1)} %ffn_hbm.1, bf16[128,2048]{1,0:T(8,128)(2,1)} %mix_hbm.1, f32[1,2048]{1,0:T(1,128)} %bitcast.14, f32[1,2048]{1,0:T(1,128)} %bitcast.15, f32[1,512]{1,0:T(1,128)} %bitcast.17, f32[1,2048]{1,0:T(1,128)} %bitcast.16, ...), custom_call_target="tpu_custom_call" | custom-call | tf_op jit(solution)/shard_map/layer/pallas_call | solution.py:822
  51.5 0.7 %copy.23 = bf16[32,2048]{1,0:T(8,128)(2,1)} copy(bf16[32,2048]{1,0:T(8,128)(2,1)S(1)} %get-tuple-element.2) | data formatting | bytes 262144
  52.2 0.7 %copy.24 = bf16[32,2048]{1,0:T(8,128)(2,1)} copy(bf16[32,2048]{1,0:T(8,128)(2,1)S(1)} %get-tuple-element.3) | data formatting | bytes 262144

commit v3 on v2

--- a/solution.py
+++ b/solution.py
@@ -220,50 +220,27 @@
 
 MESH = pl.DeviceIdType.MESH
 PIECES = 2
+NAMES = (
+    "A0", "A1", "A2", "A3", "C00", "C01", "CH", "D10", "D11", "D20", "D21", "D30", "D31", "E0", "E1", "E2", "E3",
+    "FH", "FM", "LC0", "LD1", "LD2", "LD3", "LX0", "LX1", "LX2", "LX3", "LY0", "LY1", "LY2", "LY3", "LZ1", "LZ2",
+    "LZ3", "Lown", "P0a", "P0b", "P1a", "P1b", "P2a", "P2b", "P3a", "P3b", "PR", "Q00", "Q01", "Q10", "Q11",
+    "Q20", "Q21", "Q30", "Q31", "R00", "R01", "R10", "R11", "R20", "R21", "R30", "R31", "X0a", "X1", "X2", "X3",
+    "XY0", "Y0b", "Y1", "Y2", "Y3", "Z10", "Z11", "Z20", "Z21", "Z30", "Z31", "lats", "prep", "qry",
+)
 OUTER = (
-    ["prep", "lats", "Lown", "Y0b"],
-    ["X0a", "XY0", "Z10", "Z11"],
-    ["C00", "qry", "Z20", "LZ1"],
-    ["C01", "LX0", "E0", "Z21"],
-    ["P0a", "Y1", "LY0", "D10"],
-    ["Z30", "LZ2", "X1", "D11"],
-    ["LC0", "E1", "Z31", "LY1"],
-    ["P1a", "D20", "X2", "Y2"],
-    ["P0b", "D21", "R00", "E2"],
-    ["LX2", "P1b", "P2a", "D30"],
-    ["LZ3", "Y3", "LY2", "X3"],
-    ["P2b", "LD1", "D31", "A0"],
-    ["LD2", "LX1", "R20", "E3"],
-    ["R10", "LD3", "R21", "LY3"],
-    ["P3a", "R11", "Q20", "A2"],
-    ["Q21", "LX3", "A1", "Q10"],
-    ["P3b", "R30", "R01", "A3"],
-    ["R31", "PR", "Q00", "Q11"],
-    ["Q30", "CH", "Q31", "Q01"],
-    ["FH", "FM"],
+    76, 75, 60, 34, 77, 65, 69, 4, 70, (1, 35), 5, 64, 23, 71, (4, 34), 13, (6, 23), 19, 7, 27, 72, (8, 21), 73,
+    61, 66, (8, 53), 8, 31, (12, 53), 74, 14, 0, 37, 38, 62, 9, 54, 67, 55, 10, (22, 24), 68, 63, (22, 15), 15,
+    32, 11, (25, 18), 12, 33, 39, 40, 28, 56, 20, 57, 16, 24, (35, 46), 41, 46, 29, 35, 25, 22, 26, 30, 1, 42, 21,
+    48, 3, 58, 47, 2, 59, 43, 36, 52, (48, 39), 50, 6, (57, 46), 51, 49, 53, (57, 45), 44, (66, 96), 17, (69, 40),
+    45, 18,
 )
 INNER = (
-    ["prep", "lats", "Lown", "Y0b"],
-    ["X0a", "Z10", "Z20", "Z11"],
-    ["XY0", "Z21", "LZ2", "C00"],
-    ["LZ1", "LX0", "Z30", "C01"],
-    ["LY0", "E0", "D10", "Z31"],
-    ["Y1", "D20", "D11", "X1"],
-    ["LY2", "LX2", "Y2", "X2"],
-    ["P0a", "D21", "LZ3", "LC0"],
-    ["D30", "E1", "LY1", "E2"],
-    ["P1a", "P2a", "P2b", "LY3"],
-    ["LD1", "P1b", "D31", "X3"],
-    ["qry", "R10", "Y3", "A0"],
-    ["LD2", "R20", "E3", "LD3"],
-    ["LX3", "R21", "R11", "P0b"],
-    ["A2", "P3a", "LX1", "Q20"],
-    ["Q21", "P3b", "A3", "A1"],
-    ["R30", "Q10", "R31", "PR"],
-    ["R00", "R01", "Q11", "Q30"],
-    ["CH", "Q31", "Q00", "Q01"],
-    ["FM", "FH"],
+    76, 75, 34, 60, 65, 71, 69, 70, 72, 32, 31, 77, 27, 4, 73, 23, 5, (2, 53), 74, 7, (5, 23), 61, 8, 66, 9, 10,
+    62, 20, 67, 14, 15, 11, 12, 64, 33, 19, 63, 37, 25, 38, 39, 40, 68, 26, 30, 16, 56, 22, 21, 13, 54, 41, 55,
+    42, 29, 57, 28, 24, 0, 3, (34, 27), 58, 48, 46, 2, 1, 47, 59, 43, 35, 50, 6, 36, (50, 29), 51, (50, 49), 52,
+    (52, 71), 17, 49, 53, (67, 36), 44, (68, 74), 45, (72, 53), 18,
 )
+CROSS = (1, 2)
 
 
 def flip(value, bits):
@@ -284,11 +261,19 @@
     return {"ep": z * 2 + x, "tp": y * 2 + core}
 
 
-def greet(partners):
+def greet(partners, extra, has_extra):
     barrier = pltpu.get_barrier_semaphore()
     for partner in partners:
         pl.semaphore_signal(barrier, inc=1, device_id=partner, device_id_type=MESH)
-    pl.semaphore_wait(barrier, len(partners))
+
+    @pl.when(has_extra)
+    def _():
+        pl.semaphore_signal(barrier, inc=1, device_id=extra, device_id_type=MESH)
+        pl.semaphore_wait(barrier, len(partners) + 1)
+
+    @pl.when(jnp.logical_not(has_extra))
+    def _():
+        pl.semaphore_wait(barrier, len(partners))
 
 
 def layer_kernel(
@@ -296,12 +281,12 @@
     ffn_hbm, mix_hbm, ffn_gain_hbm, mix_gain_hbm, latent_gain_hbm, out_gain_hbm, routes_hbm, scores_hbm,
     base_hbm, step_hbm, latent_hbm, rotary_hbm, query_hbm, gate_hbm, up_hbm, down_hbm, key_hbm,
     value_hbm, output_hbm, mixed_ref, moe_ref,
-    rows_all, lat_all, part_ref, work, twin_in, hop_in, direct_in, relay_in, column_in,
+    rows_all, lat_all, part_ref, work, twin_in, hop_in, direct_in, relay_in, column_in, corner_in,
     heads_ref, heads_work, heads_twin, heads_in, query_ref, keys, values, weighted, totals, attended, own_total,
     table_ref, turn_ref, ffn_ref, mix_ref,
     ffn_gain, mix_gain, latent_gain, gain_ref, routes_ref, scores_ref, base_ref, step_ref, latent_ref,
     rotary_ref, query_w, gate_ref, up_ref, down_ref, key_ref, value_ref, output_ref,
-    row_send, row_recv, lat_send, lat_recv, send_sem, twin_sem, square_sem, column_sem, heads_sem, load_sem,
+    row_send, row_recv, lat_send, lat_recv, send_sem, twin_sem, square_sem, column_sem, corner_sem, heads_sem, load_sem,
 ):
     f32, bf16 = jnp.float32, jnp.bfloat16
     ep, tp = lax.axis_index("ep"), lax.axis_index("tp")
@@ -339,9 +324,9 @@
             loads[waited[0]].wait()
             waited[0] += 1
 
-    greet([place(p, x, y, core) for p in planes[1:]] + [x_next, y_next, twin])
+    greet([z_out, x_next, y_next, twin], z_in, inner == 1)
     always = None
-    issued = {}
+    issued, settled, now = {}, set(), [0]
 
     def guarded(condition, action):
         if condition is None:
@@ -356,7 +341,7 @@
             if role[0] == "outer":
                 return
             condition = always if role[0] == "inner" else is_inner
-        issued.setdefault(key, (build, condition))
+        issued.setdefault(key, (build, condition, now[0]))
         guarded(condition, lambda: build().start())
 
     numbers = {}
@@ -567,11 +552,24 @@
 
     def sum_pairs(s, corner):
         a, b = (1, 1) if corner else (0, 1) if s % 2 else (1, 0)
-        landing, which = (hop_in, 0) if corner else (direct_in, 1)
-        work[s, a, b] = paired(s, a, b).astype(bf16)
+        value = paired(s, a, b)
+        if corner and s == 0 and CROSS:
+            for n in (1,) if role[0] == "outer" else (1, 2, 3):
+                for g in range(PIECES):
+                    arrive(corner_in.at[planes[n], rows_of(g)], corner_sem.at[planes[n], g])
+                value = value + corner_in[planes[n]].astype(f32)
+        work[s, a, b] = value.astype(bf16)
         for g in range(PIECES):
+            rows = rows_of(g)
+            if corner and s in CROSS:
+                send(
+                    work.at[s, a, b, rows], corner_in.at[z, rows], corner_sem.at[z, g],
+                    place(planes[s], x, y, core), "corner", s, g,
+                )
+                continue
+            landing, which = (hop_in, 0) if corner else (direct_in, 1)
             send(
-                work.at[s, a, b, rows_of(g)], landing.at[s, rows_of(g)], square_sem.at[which, s, g],
+                work.at[s, a, b, rows], landing.at[s, rows], square_sem.at[which, s, g],
                 y_next if s % 2 else x_next, which, s, g,
             )
 
@@ -579,8 +577,10 @@
         a, b = (1, 0) if s % 2 else (0, 1)
         rows = rows_of(g)
         value = paired(s, a, b, g)
-        arrive(hop_in.at[s, rows], square_sem.at[0, s, g])
-        work[s, a, b, rows] = (value + hop_in[s, rows].astype(f32)).astype(bf16)
+        if s not in CROSS:
+            arrive(hop_in.at[s, rows], square_sem.at[0, s, g])
+            value = value + hop_in[s, rows].astype(f32)
+        work[s, a, b, rows] = value.astype(bf16)
         send(
             work.at[s, a, b, rows], relay_in.at[s, rows], square_sem.at[2, s, g],
             x_next if s % 2 else y_next, 2, s, g,
@@ -769,23 +769,42 @@
             kind = step.rstrip("0123456789")
             kinds[kind](*(int(digit) for digit in step[len(kind) :]))
 
-    orders = [sum(order, []) for order in (OUTER, INNER)]
+    def settle(until, most):
+        ready = [k for k, (_, _, step) in issued.items() if k not in settled and step <= until]
+        for key in ready[:most]:
+            build, condition, _ = issued[key]
+            guarded(condition, lambda: build().wait_send())
+            settled.add(key)
+
+    def walk(order):
+        for step in order:
+            if isinstance(step, tuple):
+                settle(*step)
+            else:
+                run(NAMES[step])
+                now[0] += 1
+
+    orders = (OUTER, INNER)
     shared = 0
     while orders[0][shared] == orders[1][shared]:
-        run(orders[0][shared])
         shared += 1
-    ready, sent = waited[0], dict(issued)
+    walk(orders[0][:shared])
+    ready, sent, step_now, done = waited[0], dict(issued), now[0], set(settled)
     for name, chosen, order in (("outer", is_outer, orders[0]), ("inner", is_inner, orders[1])):
-        role[0], waited[0] = name, ready
+        role[0], waited[0], now[0] = name, ready, step_now
         issued.clear()
         issued.update(sent)
+        settled.clear()
+        settled.update(done)
 
         @pl.when(chosen)
         def _():
-            for step in order[shared:]:
-                run(step)
-            for build, condition in issued.values():
-                guarded(condition, lambda: build().wait_send())
+            walk(order[shared:])
+            settle(now[0], len(issued))
+
+
+def scoped_kernel(width, heads, sems, *refs):
+    pl.run_scoped(lambda *held: layer_kernel(width, heads, *refs, *held), *sems)
 
 
 def turn_tables(row_count, experts):
@@ -819,8 +838,13 @@
     scratch = lambda *shape: pltpu.VMEM(shape, jnp.bfloat16)
     wide = lambda *shape: pltpu.VMEM(shape, jnp.float32)
     sems = lambda *shape: pltpu.SemaphoreType.DMA(shape)
+    semaphores = (
+        sems(96), sems(experts, parts, PIECES), sems(48), sems(experts, parts), sems(64),
+        sems(depth, 2, 2), sems(3, depth, PIECES), sems(depth, PIECES), sems(depth, PIECES), sems(3),
+        sems(len(operands)),
+        )
     return pl.pallas_call(
-        functools.partial(layer_kernel, width, heads),
+        functools.partial(scoped_kernel, width, heads, semaphores),
         out_shape=[pltpu.VMEM((quarter, width), jnp.bfloat16)] * 2,
         in_specs=[pl.BlockSpec(memory_space=pl.ANY)] * len(operands),
         out_specs=[pl.BlockSpec(memory_space=pltpu.VMEM)] * 2,
@@ -828,7 +852,7 @@
             scratch(experts, parts, quarter, width + 2 * ROPE),
             scratch(experts, parts, quarter, latent_weight.shape[1]),
             held(depth, 2, parts), held(depth, 2, 2), held(depth, 2, 2),
-            held(depth), held(depth), held(depth), held(depth),
+            held(depth), held(depth), held(depth), held(depth), held(depth),
             held(parts), held(), held(2), held(),
             scratch(heads, row_count, NOPE + 2 * ROPE), scratch(heads, block_rows, NOPE + 2 * ROPE),
             scratch(heads, block_rows, VD), wide(heads, row_count, VD), wide(heads, row_count, VD),
@@ -836,11 +860,7 @@
             wide(row_count, 2 * ROPE), wide(row_count, 2 * ROPE),
             pltpu.VMEM((quarter, width), ffn_in.dtype), pltpu.VMEM(mix_in.shape, mix_in.dtype),
         ]
-        + [pltpu.VMEM(a.shape, a.dtype) for a in operands[2:]]
-        + [
-            sems(96), sems(experts, parts, PIECES), sems(48), sems(experts, parts), sems(64),
-            sems(depth, 2, 2), sems(3, depth, PIECES), sems(depth, PIECES), sems(3), sems(len(operands)),
-        ],
+        + [pltpu.VMEM(a.shape, a.dtype) for a in operands[2:]],
         compiler_params=pltpu.CompilerParams(
             collective_id=0, has_side_effects=True, vmem_limit_bytes=60 * 1024 * 1024
         ),

time: 53 us -> 46.8 us (0.88)
  Pallas kernels: 50.9 us -> 44.7 us
    pallas_call x1, Pallas kernels: 50.9 us -> 44.7 us  [dense_local(): pl.pallas_call(functools.partial(scoped_kernel, width, heads, semaphores)...]
where the time goes in v3:
time: 46.8 us; the launch traced here: 46.7 us
  Pallas kernels  44.7 us (96%)
  local copies, waits for them, and re-layouts  1.31 us (3%)
  between operations  0.65 us (1%)
    pallas_call x1, Pallas kernels, dense_local(): pl.pallas_call(functools.partial(scoped_kernel, width, heads, semaphores)...  44.7 us
    unnamed x2, local copies, waits for them, and re-layouts  1.31 us

profile of v3, /device:TPU:0, one launch (start us, length us, event | category | flops | bytes accessed | tf_op | source)
XLA Modules:
  0.0 46.7 jit_solution(2664628895895115437)
XLA Ops:
  0.6 44.7 %layer.1 = (bf16[32,2048]{1,0:T(8,128)(2,1)S(1)}, bf16[32,2048]{1,0:T(8,128)(2,1)S(1)}) custom-call(bf16[128,2048]{1,0:T(8,128)(2,1)} %refs_0_.1, bf16[128,2048]{1,0:T(8,128)(2,1)} %refs_1_.1, f32[1,2048]{1,0:T(1,128)} %bitcast.14, f32[1,2048]{1,0:T(1,128)} %bitcast.15, f32[1,512]{1,0:T(1,128)} %bitcast.17, f32[1,2048]{1,0:T(1,128)} %bitcast.16, ...), custom_call_target="tpu_custom_call" | custom-call | tf_op jit(solution)/shard_map/layer/pallas_call | solution.py:846
  45.4 0.7 %copy.23 = bf16[32,2048]{1,0:T(8,128)(2,1)} copy(bf16[32,2048]{1,0:T(8,128)(2,1)S(1)} %get-tuple-element.2) | data formatting | bytes 262144
  46.0 0.7 %copy.24 = bf16[32,2048]{1,0:T(8,128)(2,1)} copy(bf16[32,2048]{1,0:T(8,128)(2,1)S(1)} %get-tuple-element.3) | data formatting | bytes 262144

commit v4 on v3

--- a/solution.py
+++ b/solution.py
@@ -219,26 +219,30 @@
 
 
 MESH = pl.DeviceIdType.MESH
-PIECES = 2
+PIECES = 4
 NAMES = (
-    "A0", "A1", "A2", "A3", "C00", "C01", "CH", "D10", "D11", "D20", "D21", "D30", "D31", "E0", "E1", "E2", "E3",
-    "FH", "FM", "LC0", "LD1", "LD2", "LD3", "LX0", "LX1", "LX2", "LX3", "LY0", "LY1", "LY2", "LY3", "LZ1", "LZ2",
-    "LZ3", "Lown", "P0a", "P0b", "P1a", "P1b", "P2a", "P2b", "P3a", "P3b", "PR", "Q00", "Q01", "Q10", "Q11",
-    "Q20", "Q21", "Q30", "Q31", "R00", "R01", "R10", "R11", "R20", "R21", "R30", "R31", "X0a", "X1", "X2", "X3",
-    "XY0", "Y0b", "Y1", "Y2", "Y3", "Z10", "Z11", "Z20", "Z21", "Z30", "Z31", "lats", "prep", "qry",
+    "A0", "A1", "A2", "A3", "C00", "C01", "C02", "C03", "CH", "D10", "D11", "D12", "D13", "D20", "D21", "D22",
+    "D23", "D30", "D31", "D32", "D33", "E0", "E1", "E2", "E3", "FH", "FM", "LC0", "LD1", "LD2", "LD3", "LX0",
+    "LX1", "LX2", "LX3", "LY0", "LY1", "LY2", "LY3", "LZ1", "LZ2", "LZ3", "Lown", "P0a", "P0b", "P1a", "P1b",
+    "P2a", "P2b", "P3a", "P3b", "PR", "Q00", "Q01", "Q02", "Q03", "Q10", "Q11", "Q12", "Q13", "Q20", "Q21", "Q22",
+    "Q23", "Q30", "Q31", "Q32", "Q33", "R00", "R01", "R02", "R03", "R10", "R11", "R12", "R13", "R20", "R21",
+    "R22", "R23", "R30", "R31", "R32", "R33", "X0a", "X1", "X2", "X3", "XY0", "Y0b", "Y1", "Y2", "Y3", "Z10",
+    "Z11", "Z12", "Z13", "Z20", "Z21", "Z22", "Z23", "Z30", "Z31", "Z32", "Z33", "lats", "prep", "qry",
 )
 OUTER = (
-    76, 75, 60, 34, 77, 65, 69, 4, 70, (1, 35), 5, 64, 23, 71, (4, 34), 13, (6, 23), 19, 7, 27, 72, (8, 21), 73,
-    61, 66, (8, 53), 8, 31, (12, 53), 74, 14, 0, 37, 38, 62, 9, 54, 67, 55, 10, (22, 24), 68, 63, (22, 15), 15,
-    32, 11, (25, 18), 12, 33, 39, 40, 28, 56, 20, 57, 16, 24, (35, 46), 41, 46, 29, 35, 25, 22, 26, 30, 1, 42, 21,
-    48, 3, 58, 47, 2, 59, 43, 36, 52, (48, 39), 50, 6, (57, 46), 51, 49, 53, (57, 45), 44, (66, 96), 17, (69, 40),
-    45, 18,
+    106, 105, 42, 89, 84, 93, 94, 95, 96, 4, 31, (2, 22), 5, 6, 7, 35, (2, 111), 90, 97, 98, (7, 19), 27, 9, 10,
+    88, 99, 100, 40, 101, (12, 23), 102, 107, 39, 85, 11, 12, (16, 23), 103, (21, 17), 22, 104, 91, (23, 45), 45,
+    13, 86, 14, 15, 37, 46, 72, 73, 74, 16, 75, 21, 87, 92, 23, 17, 18, 19, 20, 41, 47, 48, 76, 77, 33, 78, 79,
+    36, 32, 24, (50, 47), 49, 43, 50, 34, 60, 28, 61, 0, 62, 63, 30, 29, 56, 57, 38, 58, 59, 1, 80, 81, 3, 82, 83,
+    44, 68, 2, 69, 51, 70, 64, 65, (68, 13), 8, 66, 67, 71, (68, 182), 25, 52, 53, 54, 55, 26,
 )
 INNER = (
-    76, 75, 34, 60, 65, 71, 69, 70, 72, 32, 31, 77, 27, 4, 73, 23, 5, (2, 53), 74, 7, (5, 23), 61, 8, 66, 9, 10,
-    62, 20, 67, 14, 15, 11, 12, 64, 33, 19, 63, 37, 25, 38, 39, 40, 68, 26, 30, 16, 56, 22, 21, 13, 54, 41, 55,
-    42, 29, 57, 28, 24, 0, 3, (34, 27), 58, 48, 46, 2, 1, 47, 59, 43, 35, 50, 6, 36, (50, 29), 51, (50, 49), 52,
-    (52, 71), 17, 49, 53, (67, 36), 44, (68, 74), 45, (72, 53), 18,
+    106, 105, 42, 84, 89, 97, 93, 98, 99, 94, 100, 95, 107, 96, 40, 4, (2, 21), 5, 101, 102, 6, 31, 7, (2, 46), 9,
+    (6, 23), 10, 88, 103, 104, 13, (7, 18), 11, (8, 21), 86, 14, 91, 12, 15, 16, (10, 33), 90, 39, 35, 85, 23, 17,
+    18, 22, 47, 87, 19, 20, 33, 41, 45, 32, 37, 92, 48, 28, 46, 21, 36, 27, 24, 34, (40, 45), 49, 72, 73, 76, 30,
+    50, 29, 74, 38, 75, 77, 0, 56, (48, 20), 57, 3, 78, 79, 1, 80, 58, 59, 81, 82, 83, 2, 51, (60, 14), 64, 8, 65,
+    43, 66, 60, (65, 18), 67, 44, (70, 32), 68, (75, 21), 69, (76, 21), 70, (87, 21), 71, 61, 62, (87, 50), 52,
+    (87, 20), 53, 25, 63, 54, (93, 20), 55, (96, 20), 26,
 )
 CROSS = (1, 2)
 
@@ -269,18 +273,24 @@
     @pl.when(has_extra)
     def _():
         pl.semaphore_signal(barrier, inc=1, device_id=extra, device_id_type=MESH)
-        pl.semaphore_wait(barrier, len(partners) + 1)
-
-    @pl.when(jnp.logical_not(has_extra))
-    def _():
-        pl.semaphore_wait(barrier, len(partners))
+
+    def wait():
+        @pl.when(has_extra)
+        def _():
+            pl.semaphore_wait(barrier, len(partners) + 1)
+
+        @pl.when(jnp.logical_not(has_extra))
+        def _():
+            pl.semaphore_wait(barrier, len(partners))
+
+    return wait
 
 
 def layer_kernel(
     width, heads,
     ffn_hbm, mix_hbm, ffn_gain_hbm, mix_gain_hbm, latent_gain_hbm, out_gain_hbm, routes_hbm, scores_hbm,
     base_hbm, step_hbm, latent_hbm, rotary_hbm, query_hbm, gate_hbm, up_hbm, down_hbm, key_hbm,
-    value_hbm, output_hbm, mixed_ref, moe_ref,
+    value_hbm, output_hbm, out_ref,
     rows_all, lat_all, part_ref, work, twin_in, hop_in, direct_in, relay_in, column_in, corner_in,
     heads_ref, heads_work, heads_twin, heads_in, query_ref, keys, values, weighted, totals, attended, own_total,
     table_ref, turn_ref, ffn_ref, mix_ref,
@@ -315,7 +325,9 @@
         (key_hbm, key_ref), (value_hbm, value_ref), (output_hbm, output_ref), (out_gain_hbm, gain_ref),
     )
     loads = [pltpu.make_async_copy(src, dst, load_sem.at[n]) for n, (src, dst) in enumerate(copied)]
-    for load in loads:
+    greeted = greet([z_out, x_next, y_next, twin], z_in, inner == 1)
+    early = 11
+    for load in loads[:early]:
         load.start()
     waited = [0]
 
@@ -324,7 +336,6 @@
             loads[waited[0]].wait()
             waited[0] += 1
 
-    greet([z_out, x_next, y_next, twin], z_in, inner == 1)
     always = None
     issued, settled, now = {}, set(), [0]
 
@@ -730,7 +741,7 @@
         projected = (
             heads_ref[y * 2 + core].astype(f32) + heads_twin[0].astype(f32) + heads_in[...].astype(f32)
         )
-        mixed_ref[...] = rms_rows(projected, gain_ref[...]).astype(bf16)
+        out_ref[0] = rms_rows(projected, gain_ref[...]).astype(bf16)
 
     def finish_moe():
         for g in range(PIECES):
@@ -739,16 +750,19 @@
             for s in range(1, depth):
                 arrive(column_in.at[planes[s], rows], column_sem.at[planes[s], g])
                 total = total + column_in[planes[s], rows].astype(f32)
-            moe_ref[rows, :] = total.astype(bf16)
+            out_ref[1, rows, :] = total.astype(bf16)
 
     def start_rows():
         prepare_rows()
+        greeted()
         own_rows()
+        for load in loads[early:]:
+            load.start()
 
     steps = {
         "prep": start_rows, "lats": prepare_lats, "qry": prepare_queries, "Lown": own_lats,
         "X0a": lambda: side_rows("x"), "Y0b": lambda: side_rows("y"), "XY0": side_rows_rest,
-        "C00": lambda: corner_rows(0), "C01": lambda: corner_rows(1),
+        **{f"C0{g}": functools.partial(corner_rows, g) for g in range(PIECES)},
         "LX0": lambda: side_lats(1), "LY0": lambda: side_lats(0), "LC0": corner_lats,
         "PR": project, "CH": cross_heads, "FH": finish_heads, "FM": finish_moe,
     }
@@ -839,15 +853,15 @@
     wide = lambda *shape: pltpu.VMEM(shape, jnp.float32)
     sems = lambda *shape: pltpu.SemaphoreType.DMA(shape)
     semaphores = (
-        sems(96), sems(experts, parts, PIECES), sems(48), sems(experts, parts), sems(64),
+        sems(160), sems(experts, parts, PIECES), sems(48), sems(experts, parts), sems(128),
         sems(depth, 2, 2), sems(3, depth, PIECES), sems(depth, PIECES), sems(depth, PIECES), sems(3),
         sems(len(operands)),
         )
-    return pl.pallas_call(
+    both = pl.pallas_call(
         functools.partial(scoped_kernel, width, heads, semaphores),
-        out_shape=[pltpu.VMEM((quarter, width), jnp.bfloat16)] * 2,
+        out_shape=pltpu.VMEM((2, quarter, width), jnp.bfloat16),
         in_specs=[pl.BlockSpec(memory_space=pl.ANY)] * len(operands),
-        out_specs=[pl.BlockSpec(memory_space=pltpu.VMEM)] * 2,
+        out_specs=pl.BlockSpec(memory_space=pltpu.VMEM),
         scratch_shapes=[
             scratch(experts, parts, quarter, width + 2 * ROPE),
             scratch(experts, parts, quarter, latent_weight.shape[1]),
@@ -866,6 +880,7 @@
         ),
         name="layer",
     )(*operands)
+    return both[0], both[1]
 
 
 def solution(mesh):
@@ -874,7 +889,7 @@
     def body(*args):
         quarter, choose = args[10].shape[0] // parts, args[15].shape[1]
         every_row = 2 * quarter * choose >= quarter * experts
-        paired = parts == 4 and experts == 8 and quarter % (16 * PIECES) == 0
+        paired = parts == 4 and experts == 8 and quarter % (8 * PIECES) == 0
         return (dense_local if every_row and paired else local)(*args)
     placed = (
         P("ep", None),

time: 46.8 us -> 45.8 us (0.979)
  local copies, waits for them, and re-layouts: 1.31 us -> 0.72 us
    unnamed x2 -> x0, local copies, waits for them, and re-layouts: 1.31 us -> none
    squeeze x0 -> x1, local copies, waits for them, and re-layouts: none -> 0.72 us  [dense_local(): return (both[0], both[1])]
where the time goes in v4:
time: 45.8 us; the launch traced here: 45.6 us
  Pallas kernels  44.3 us (97%)
  local copies, waits for them, and re-layouts  0.72 us (2%)
  between operations  0.65 us (1%)
    pallas_call x1, Pallas kernels, dense_local(): pl.pallas_call(functools.partial(scoped_kernel, width, heads, semaphores)...  44.3 us

profile of v4, /device:TPU:0, one launch (start us, length us, event | category | flops | bytes accessed | tf_op | source)
XLA Modules:
  0.0 45.6 jit_solution(2902816888381195156)
XLA Ops:
  0.6 44.3 %layer.1 = bf16[2,32,2048]{2,1,0:T(8,128)(2,1)S(1)} custom-call(bf16[128,2048]{1,0:T(8,128)(2,1)} %refs_0_.1, bf16[128,2048]{1,0:T(8,128)(2,1)} %refs_1_.1, f32[1,2048]{1,0:T(1,128)} %bitcast.18, f32[1,2048]{1,0:T(1,128)} %bitcast.19, f32[1,512]{1,0:T(1,128)} %bitcast.21, f32[1,2048]{1,0:T(1,128)} %bitcast.20, s32[4,128]{1,0:T(4,128)} %bitcast.22, ...), custom_call_target="tpu_custom_call" | custom-call | tf_op jit(solution)/shard_map/layer/pallas_call | solution.py:860
  44.9 0.7 %slice_bitcast_fusion = (bf16[32,2048]{1,0:T(8,128)(2,1)}, bf16[32,2048]{1,0:T(8,128)(2,1)}) fusion(bf16[2,32,2048]{2,1,0:T(8,128)(2,1)S(1)} %layer.1), kind=kLoop, calls=%fused_computation | loop fusion | bytes 524288 | tf_op jit(solution)/shard_map/squeeze | solution.py:883

commit v5 on v4

--- a/solution.py
+++ b/solution.py
@@ -531,23 +531,26 @@
 
     def expert_plane(s):
         loaded(15)
-        for a in (0, 1):
-            for b in (0, 1):
-                take_row(place(planes[s], flip(x, a), flip(y, b), 1 - core), None)
-        pair = pl.ds(planes[s] * 2, 2)
-        block = rows_all[pair, :, :, :width].reshape(block_rows, width)
+        for a in (1, 0):
+            expert_half(s, a)
+
+    def expert_half(s, a):
+        for b in (0, 1):
+            take_row(place(planes[s], flip(x, a), flip(y, b), 1 - core), None)
+        e = planes[s] * 2 + flip(x, a)
+        block = rows_all[e, :, :, :width].reshape(row_count, width)
         gate_part = jnp.dot(block, gate_ref[...], preferred_element_type=f32)
         up_part = jnp.dot(block, up_ref[...], preferred_element_type=f32)
         hidden = clamped_unit(gate_part, up_part).astype(bf16)
-        table = rows_all[pair, :, :, width:].reshape(block_rows, 2 * ROPE)
+        table = rows_all[e, :, :, width:].reshape(row_count, 2 * ROPE)
         lane = lax.broadcasted_iota(jnp.int32, table.shape, 1)
         is_mine = (lane == ROPE + ep) | (lane == ROPE + experts + ep)
         share = jnp.sum(jnp.where(is_mine, table.astype(f32), 0.0), axis=1, keepdims=True)
         chunk = 512
         for n in range(0, width, chunk):
             out = jnp.dot(hidden, down_ref[:, n : n + chunk], preferred_element_type=f32) * share
-            part_ref[s, :, :, :, n : n + chunk] = out.astype(bf16).reshape(2, parts, quarter, chunk)
-        for a, b in ((1, 1), (0, 1), (1, 0), (0, 0)) if s % 2 else ((1, 1), (1, 0), (0, 1), (0, 0)):
+            part_ref[s, flip(x, a), :, :, n : n + chunk] = out.astype(bf16).reshape(parts, quarter, chunk)
+        for b in (1, 0):
             mine = part_ref.at[s, flip(x, a), flip(y, b) * 2 + 1 - core]
             send(mine, twin_in.at[s, a, b], twin_sem.at[s, a, b], twin, "twin", s, a, b)
 

time: 45.8 us -> 45.3 us (0.989)
  Pallas kernels: 44.3 us -> 43.8 us
    pallas_call x1, Pallas kernels: 44.3 us -> 43.8 us  [dense_local(): pl.pallas_call(functools.partial(scoped_kernel, width, heads, semaphores)...]
where the time goes in v5:
time: 45.3 us; the launch traced here: 45.1 us
  Pallas kernels  43.8 us (97%)
  local copies, waits for them, and re-layouts  0.72 us (2%)
  between operations  0.65 us (1%)
    pallas_call x1, Pallas kernels, dense_local(): pl.pallas_call(functools.partial(scoped_kernel, width, heads, semaphores)...  43.8 us

profile of v5, /device:TPU:0, one launch (start us, length us, event | category | flops | bytes accessed | tf_op | source)
XLA Modules:
  0.0 45.1 jit_solution(14365526247838284008)
XLA Ops:
  0.6 43.8 %layer.1 = bf16[2,32,2048]{2,1,0:T(8,128)(2,1)S(1)} custom-call(bf16[128,2048]{1,0:T(8,128)(2,1)} %refs_0_.1, bf16[128,2048]{1,0:T(8,128)(2,1)} %refs_1_.1, f32[1,2048]{1,0:T(1,128)} %bitcast.18, f32[1,2048]{1,0:T(1,128)} %bitcast.19, f32[1,512]{1,0:T(1,128)} %bitcast.21, f32[1,2048]{1,0:T(1,128)} %bitcast.20, s32[4,128]{1,0:T(4,128)} %bitcast.22, ...), custom_call_target="tpu_custom_call" | custom-call | tf_op jit(solution)/shard_map/layer/pallas_call | solution.py:863
  44.4 0.7 %slice_bitcast_fusion = (bf16[32,2048]{1,0:T(8,128)(2,1)}, bf16[32,2048]{1,0:T(8,128)(2,1)}) fusion(bf16[2,32,2048]{2,1,0:T(8,128)(2,1)S(1)} %layer.1), kind=kLoop, calls=%fused_computation | loop fusion | bytes 524288 | tf_op jit(solution)/shard_map/squeeze | solution.py:886
